TPU v7x, 512 devices: a whole 4x8x8 slice. The times are simulated.
512 devices in a mesh: sp: 32 (over z, x), tp: 16 (over y, core).
Axes of the slice: x: 4, y: 8, z: 8, core: 2. Of those that a mesh axis runs over, the one named last changes fastest.
Arguments:
- target_rows: bfloat16 [2048, 2048], P(('sp', 'tp')), may hold values from -6 to 6
- source_rows: bfloat16 [8192, 2048], P(('sp', 'tp')), may hold values from -6 to 6
- norm_gain: bfloat16 [2048], replicated, may hold values from 0.099609375 to 1.8984375
- query_weight: bfloat16 [2048, 4096], P(None, 'tp'), may hold values from -0.125 to 0.125
- key_weight: bfloat16 [2048, 4096], P(None, 'tp'), may hold values from -0.125 to 0.125
- value_weight: bfloat16 [2048, 4096], P(None, 'tp'), may hold values from -0.125 to 0.125
- output_weight: bfloat16 [4096, 2048], P('tp'), may hold values from -0.09375 to 0.09375
- saved_output: bfloat16 [2048, 4096], P('sp', 'tp'), may hold values from -3 to 3
- norm_offset: bfloat16 [2048, 16], P('sp', 'tp'), may hold values from 0.25 to 1.25
- output_grad: bfloat16 [2048, 2048], P(('sp', 'tp')), may hold values from -192 to 192
Outputs:
- target_grad: float32 [2048, 2048], P(('sp', 'tp'))
- source_grad: float32 [8192, 2048], P(('sp', 'tp'))
- query_weight_grad: float32 [2048, 4096], P('sp', 'tp')
All inputs are finite; a program needn't handle non-finite values.
Results may differ from a plain program's by a relative error of at most 0.033.
Values may be sent and summed in bfloat16 or wider, within the bound.
A program may use at most 64 MiB of HBM per device.

v0:
```python
import math

import jax
import jax.numpy as jnp
from jax import lax
from jax.sharding import Mesh
from jax.sharding import PartitionSpec as P

HEAD_DIM = 256
SP = ("sp_0", "sp_1")
SP_TP = ("sp_0", "sp_1", "tp")


EPSILON = 1e-06


def from_everyone(shard, axis):
    copies = jnp.broadcast_to(shard, (lax.axis_size(axis), *shard.shape))
    return lax.all_to_all(copies, axis, split_axis=0, concat_axis=0, tiled=True)


def in_order(parts, dim):
    parts = jnp.moveaxis(parts, 0, dim)
    dims = parts.shape
    return parts.reshape(*dims[:dim], dims[dim] * dims[dim + 1], *dims[dim + 2 :])


def gathered_copies(shard, axis, dim):
    parts = from_everyone(shard, axis)
    return in_order(parts, dim)


def side_by_side(arrays, axis, dim, along):
    widths = [math.prod(a.shape[along:]) for a in arrays]
    both = jnp.concatenate(
        [a.reshape(*a.shape[:along], w) for a, w in zip(arrays, widths)], axis=along
    )
    whole = lax.all_gather(both, axis, axis=dim, tiled=True)
    parts = jnp.split(whole, [sum(widths[:k]) for k in range(1, len(widths))], axis=along)
    return tuple((b.reshape(*whole.shape[:along], *a.shape[along:]) for a, b in zip(arrays, parts)))


def sum_by_axis(shard, axes, dim):
    if not axes:
        return shard
    nearer = lax.psum_scatter(shard, axes[0], scatter_dimension=dim, tiled=True)
    return sum_by_axis(nearer, axes[1:], dim)


def cut_along(shard, dim, size):
    before, after = (shard.shape[:dim], shard.shape[dim + 1 :])
    return jnp.moveaxis(shard.reshape(*before, size, -1, *after), dim, 0)


def sum_at_owner(shard, axis, dim):
    size = lax.axis_size(axis)
    parts = lax.all_to_all(cut_along(shard, dim, size), axis, 0, 0, tiled=True)
    return jnp.sum(parts.astype(jnp.float32), axis=0)


def sum_at_owner_2(shard, axis, dim):
    size = lax.axis_size(axis)
    parts = lax.all_to_all(cut_along(shard, dim, size), axis, 0, 0, tiled=True)
    return jnp.sum(parts, axis=0)


def contract_last(left, right):
    return lax.dot_general(
        left, right, (((1,), (1,)), ((), ())), preferred_element_type=jnp.float32
    )


def attention_weights(
    query_rows, head_gradient, offsets, deltas, key_row_block, value_row_block, shift_base
):
    score_scale = HEAD_DIM ** (-0.5)
    score_matrix = jnp.einsum(
        "rfo,kfo->frk", query_rows, key_row_block, preferred_element_type=jnp.float32
    )
    shifts = jnp.transpose(shift_base + offsets.astype(jnp.float32))[:, :, None]
    prob_rows = jnp.exp(score_matrix * score_scale - shifts)
    prob_grad = jnp.einsum(
        "rfo,kfo->frk", head_gradient, value_row_block, preferred_element_type=jnp.float32
    )
    score_grad = (
        prob_rows
        * (prob_grad - jnp.transpose(deltas.astype(jnp.float32))[:, :, None])
        * score_scale
    )
    return (prob_rows.astype(jnp.bfloat16), score_grad.astype(jnp.bfloat16))


def body(
    target_rows,
    source_rows,
    norm_gain,
    query_weight,
    key_weight,
    value_weight,
    output_weight,
    saved_output,
    norm_offset,
    output_grad,
):
    tp_count = lax.axis_size("tp")
    sp_count = lax.axis_size(SP)
    query_width = query_weight.shape[1]
    local_heads = query_width // HEAD_DIM
    target_count = saved_output.shape[0]
    source_count = source_rows.shape[0] * tp_count
    shift_base = math.log(source_count * sp_count)
    target_float = target_rows.astype(jnp.float32)
    gain_float = norm_gain.astype(jnp.float32)
    inverse = lax.rsqrt(jnp.mean(target_float * target_float, axis=1, keepdims=True) + EPSILON)
    normed = (target_float * inverse * gain_float).astype(jnp.bfloat16)
    slice_share = lax.all_gather(jnp.stack([normed, output_grad]), "tp", axis=1, tiled=True)
    query_part = jnp.dot(slice_share[0], query_weight, preferred_element_type=jnp.float32).astype(
        jnp.bfloat16
    )
    grad_part = contract_last(slice_share[1], output_weight).astype(jnp.bfloat16)
    joined = jnp.concatenate([query_part, grad_part, slice_share[0]], axis=1)
    query_rows = joined[:, :query_width].reshape(target_count, local_heads, HEAD_DIM)
    head_gradient = joined[:, query_width : 2 * query_width].reshape(
        target_count, local_heads, HEAD_DIM
    )
    normed_all = joined[:, 2 * query_width :]
    saved_heads = saved_output.reshape(target_count, local_heads, HEAD_DIM)
    deltas = jnp.sum(
        head_gradient.astype(jnp.float32) * saved_heads.astype(jnp.float32), axis=2
    ).astype(jnp.bfloat16)
    slice_share = gathered_copies(source_rows, "tp", 0)
    key_part = jnp.dot(slice_share, key_weight, preferred_element_type=jnp.float32).astype(
        jnp.bfloat16
    )
    value_part = jnp.dot(slice_share, value_weight, preferred_element_type=jnp.float32).astype(
        jnp.bfloat16
    )
    projected = jnp.concatenate([key_part, value_part], axis=1)
    key_row_block = projected[:, :query_width].reshape(source_count, local_heads, HEAD_DIM)
    value_row_block = projected[:, query_width:].reshape(source_count, local_heads, HEAD_DIM)
    slice_share = side_by_side((query_rows, head_gradient, norm_offset, deltas), SP, 0, 2)
    probability_rounded, score_rounded = attention_weights(
        slice_share[0],
        slice_share[1],
        slice_share[2],
        slice_share[3],
        key_row_block,
        value_row_block,
        shift_base,
    )
    key_total = jnp.einsum(
        "wcu,cwp->uwp", score_rounded, slice_share[0], preferred_element_type=jnp.float32
    )
    value_total = jnp.einsum(
        "wcu,cwp->uwp", probability_rounded, slice_share[1], preferred_element_type=jnp.float32
    )
    key_total, value_total, score_rounded = (key_total, value_total, score_rounded)
    query_term = jnp.einsum(
        "tje,etq->jtq", score_rounded, key_row_block, preferred_element_type=jnp.float32
    )
    query_grad = sum_by_axis(query_term.astype(jnp.bfloat16), SP, 0).astype(jnp.float32)
    query_flat = query_grad.astype(jnp.bfloat16).reshape(target_count, query_width)
    normed_grad = sum_at_owner(
        contract_last(query_flat, query_weight).astype(jnp.bfloat16), "tp", 0
    )
    scaled = normed_grad * gain_float
    target_grad = inverse * scaled - target_float * inverse**3 * jnp.mean(
        scaled * target_float, axis=1, keepdims=True
    )
    key_flat = key_total.astype(jnp.bfloat16).reshape(source_count, query_width)
    value_flat = value_total.astype(jnp.bfloat16).reshape(source_count, query_width)
    key_part = contract_last(key_flat, key_weight)
    value_part = contract_last(value_flat, value_weight)
    source_grad = sum_at_owner((key_part + value_part).astype(jnp.bfloat16), "tp", 0)
    weight_grad = sum_at_owner_2(
        lax.dot_general(
            normed_all, query_flat, (((0,), (0,)), ((), ())), preferred_element_type=jnp.float32
        ),
        SP,
        0,
    )
    return (target_grad, source_grad, weight_grad)


def solution(mesh):
    split = Mesh(mesh.devices.reshape(8, 4, mesh.shape["tp"]), ("sp_0", "sp_1", "tp"))
    placed = (
        P(SP_TP, None),
        P(SP_TP, None),
        P(),
        P(None, "tp"),
        P(None, "tp"),
        P(None, "tp"),
        P("tp", None),
        P(SP, "tp"),
        P(SP, "tp"),
        P(SP_TP, None),
    )
    return jax.shard_map(
        body,
        mesh=split,
        in_specs=placed,
        out_specs=(P(SP_TP, None), P(SP_TP, None), P(SP, "tp")),
        check_vma=False,
    )
```

profile of v0, /device:TPU:1, one launch (start us, length us, event | category | flops | bytes accessed | tf_op | source)
XLA Modules:
  0.0 284.2 jit_solution(7998154061447127349)
XLA Ops:
  7.2 1.0 fusion.13
  8.2 0.7 convert_element_type.117
  8.9 0.8 fusion.21
  9.7 0.8 pad_maximum_fusion.1
  10.6 0.8 copy.28
  11.4 22.4 %all_gather.6 = bf16[2,64,2048]{2,0,1:T(2,128)(2,1)S(1)} all-gather(bf16[2,4,2048]{2,0,1:T(2,128)(2,1)S(1)} %copy.25), channel_id=1, replica_groups=mesh['sp_0'=8,'sp_1'=4,'tp'=16] {'tp'}, dimensions={1}, use_global_device_ids=true | all-gather | bytes 557056 | tf_op jit(solution)/shard_map/all_gather | solution.py:116
  33.8 1.6 fusion.22
  36.1 1.5 fusion.10
  37.6 0.7 pad_maximum_fusion
  38.5 31.5 %all_to_all.20 = bf16[16,16,2048]{2,1,0:T(8,128)(2,1)S(1)} all-to-all(bf16[16,16,2048]{2,1,0:T(8,128)(2,1)S(1)} %broadcast_in_dim.2), channel_id=1, replica_groups=mesh['sp_0'=8,'sp_1'=4,'tp'=16] {'tp'}, dimensions={0} | all-to-all | bytes 2097152 | tf_op jit(solution)/shard_map/all_to_all | solution.py:19
  70.5 47.7 %all-gather.2.cloned.1.call-done = bf16[2048,1,514]{2,0,1:T(8,128)(2,1)} async-done(((bf16[64,1,514]{2,0,1:T(8,128)(2,1)}), bf16[2048,1,514]{2,0,1:T(8,128)(2,1)}) %all-gather.2.cloned.1.call-update) | async-done | bytes 2105360 | tf_op jit(solution)/shard_map/all_gather | solution.py:38
  118.2 1.9 convert_reduce_fusion.1
  120.1 3.1 %fusion.3 = f32[2048,256]{1,0:T(8,128)} fusion(bf16[256,256]{1,0:T(8,128)(2,1)S(1)} %convolution_convert_fusion.5, f32[2048]{0:T(1024)S(1)} %get-tuple-element.4, bf16[2048,1,514]{2,0,1:T(8,128)(2,1)} %all-gather.2.cloned.1.call-done), kind=kOutput, calls=%fused_computation.6 | convolution fusion | flops 269484032 | bytes 3284992 | tf_op jit(solution)/shard_map/rfo,kfo->frk/dot_general | solution.py:77
  123.2 3.3 %fusion.5 = bf16[2048,256]{1,0:T(8,128)(2,1)S(1)} fusion(f32[2048,256]{1,0:T(8,128)} %fusion.3, bf16[256,2048]{1,0:T(8,128)(2,1)S(1)} %bitcast.80, bf16[2048,256]{1,0:T(8,128)(2,1)S(1)} %copy-done, f32[2048]{0:T(1024)S(1)} %get-tuple-element.3, bf16[2048,1,514]{2,0,1:T(8,128)(2,1)} %all-gather.2.cloned.1.call-done), kind=kOutput, calls=%fused_computation.9 | convolution fusion | flops 539033600 | bytes 6299648 | tf_op jit(solution)/shard_map/rfo,kfo->frk/dot_general | solution.py:82
  126.4 1.6 fusion.6
  128.0 4.0 %fusion.8 = f32[256,2048]{1,0:T(8,128)} fusion(bf16[2048,256]{1,0:T(8,128)(2,1)S(1)} %copy-done.2, bf16[2048,256]{1,0:T(8,128)(2,1)S(1)} %fusion.5, bf16[2048,1,514]{2,0,1:T(8,128)(2,1)} %all-gather.2.cloned.1.call-done), kind=kOutput, calls=%fused_computation.18 | convolution fusion | flops 536936448 | bytes 5242880 | tf_op jit(solution)/shard_map/dot_general | solution.py:68
  132.0 4.9 %fusion.4 = bf16[256,2048]{1,0:T(8,128)(2,1)} fusion(f32[256,2048]{1,0:T(8,128)} %fusion.8, bf16[2048,256]{1,0:T(8,128)(2,1)S(1)} %copy-done, f32[2048,256]{1,0:T(8,128)} %fusion.3, bf16[2048,1,514]{2,0,1:T(8,128)(2,1)} %all-gather.2.cloned.1.call-done), kind=kOutput, calls=%fused_computation.7 | convolution fusion | flops 538509312 | bytes 7340032 | tf_op jit(solution)/shard_map/dot_general | solution.py:68
  136.9 11.6 %all-to-all-start.2 = ((bf16[16,16,2048]{2,1,0:T(8,128)(2,1)}), bf16[16,16,2048]{2,1,0:T(8,128)(2,1)S(1)}, u32[]{:S(2)}, u32[]{:S(2)}) async-start(bf16[16,16,2048]{2,1,0:T(8,128)(2,1)} %bitcast.20), calls=%async_computation.3 | async-start | bytes 2097152 | tf_op jit(solution)/shard_map/all_to_all | solution.py:57
  148.6 18.2 %reduce-scatter.5.cloned.1.call-done = bf16[256,1,256]{0,2,1:T(8,128)(2,1)} async-done(((bf16[2048,1,256]{0,2,1:T(8,128)(2,1)}), bf16[256,1,256]{0,2,1:T(8,128)(2,1)}) %reduce-scatter.5.cloned.1.call-update) | async-done | bytes 131088 | tf_op jit(solution)/shard_map/reduce_scatter | solution.py:46
  166.9 1.7 copy.36
  168.5 28.1 %reduce-scatter.7.cloned.1.call-done = bf16[64,256]{1,0:T(8,128)(2,1)} async-done(((bf16[256,256]{1,0:T(8,128)(2,1)}), bf16[64,256]{1,0:T(8,128)(2,1)}) %reduce-scatter.7.cloned.1.call-update) | async-done | bytes 32784 | tf_op jit(solution)/shard_map/reshape | solution.py:162
  196.7 1.3 convolution_convert_fusion.1
  197.9 0.8 reshape.145
  198.7 9.7 %all-to-all-start.1 = ((bf16[16,4,2048]{2,1,0:T(4,128)(2,1)}), bf16[16,4,2048]{2,1,0:T(4,128)(2,1)S(1)}, u32[]{:S(2)}, u32[]{:S(2)}) async-start(bf16[16,4,2048]{2,1,0:T(4,128)(2,1)} %reshape.145), calls=%async_computation.2 | async-start | bytes 524288 | tf_op jit(solution)/shard_map/all_to_all | solution.py:57
  208.4 1.4 copy.40
  209.9 1.8 fusion.19
  211.6 8.4 %all-to-all-done.1 = bf16[16,4,2048]{2,1,0:T(4,128)(2,1)S(1)} async-done(((bf16[16,4,2048]{2,1,0:T(4,128)(2,1)}), bf16[16,4,2048]{2,1,0:T(4,128)(2,1)S(1)}, u32[]{:S(2)}, u32[]{:S(2)}) %all-to-all-start.1) | async-done | bytes 262176 | tf_op jit(solution)/shard_map/all_to_all | solution.py:57
  220.0 8.4 %all-to-all-start.3 = ((f32[32,64,256]{2,1,0:T(8,128)}), f32[32,64,256]{2,1,0:T(8,128)S(1)}, u32[]{:S(2)}, u32[]{:S(2)}) async-start(f32[32,64,256]{2,1,0:T(8,128)} %fusion.19), calls=%async_computation.4 | async-start | bytes 4194304 | tf_op jit(solution)/shard_map/all_to_all | solution.py:63
  228.4 2.0 convert_reduce_fusion
  230.7 0.7 fusion.17
  231.4 45.5 %all-to-all-done.3 = f32[32,64,256]{2,1,0:T(8,128)S(1)} async-done(((f32[32,64,256]{2,1,0:T(8,128)}), f32[32,64,256]{2,1,0:T(8,128)S(1)}, u32[]{:S(2)}, u32[]{:S(2)}) %all-to-all-start.3) | async-done | bytes 2097184 | tf_op jit(solution)/shard_map/all_to_all | solution.py:63
  276.9 0.8 reduce_sum.59
  (38 shorter events, 1.8 us)
Async XLA Ops:
  7.2 116.0 %copy-start = (bf16[2048,256]{1,0:T(8,128)(2,1)S(1)}, bf16[2048,256]{1,0:T(8,128)(2,1)}, u32[]{:S(2)}) copy-start(bf16[2048,256]{1,0:T(8,128)(2,1)} %param.15) | copy-start | bytes 3145732
  7.2 28.2 %copy-start.10 = (bf16[64,256]{1,0:T(8,128)(2,1)S(1)}, bf16[64,256]{1,0:T(8,128)(2,1)}, u32[]{:S(2)}) copy-start(bf16[64,256]{1,0:T(8,128)(2,1)} %param.17) | copy-start | bytes 98308
  7.2 28.2 %copy-start.6 = (bf16[256,2048]{1,0:T(8,128)(2,1)S(1)}, bf16[256,2048]{1,0:T(8,128)(2,1)}, u32[]{:S(2)}) copy-start(bf16[256,2048]{1,0:T(8,128)(2,1)} %param.16) | copy-start | bytes 3145732
  7.2 111.0 %all-gather.2.cloned.1.call-start = ((), (), s32[]{:S(2)}) async-start(), calls=%async_computation.6 | async-start | bytes 2703360 | tf_op jit(solution)/shard_map/all_gather | solution.py:38
  9.7 26.3 %copy-start.3 = (bf16[2048,256]{1,0:T(8,128)(2,1)S(1)}, bf16[2048,256]{1,0:T(8,128)(2,1)}, u32[]{:S(2)}) copy-start(bf16[2048,256]{1,0:T(8,128)(2,1)} %param.13) | copy-start | bytes 3145732
  33.8 4.6 %copy-start.9 = (bf16[16,2048]{1,0:T(8,128)(2,1)S(1)}, bf16[16,2048]{1,0:T(8,128)(2,1)}, u32[]{:S(2)}) copy-start(bf16[16,2048]{1,0:T(8,128)(2,1)} %param.11) | copy-start | bytes 196612
  36.1 33.9 %copy-start.1 = (bf16[2048,256]{1,0:T(8,128)(2,1)S(1)}, bf16[2048,256]{1,0:T(8,128)(2,1)}, u32[]{:S(2)}) copy-start(bf16[2048,256]{1,0:T(8,128)(2,1)} %param.14) | copy-start | bytes 3145732
  38.3 128.6 %reduce-scatter.5.cloned.1.call-start = ((), (), s32[]{:S(2)}) async-start(), calls=%async_computation.7 | async-start | bytes 1179648 | tf_op jit(solution)/shard_map/reduce_scatter | solution.py:46
  126.4 1.6 copy-start.2
  136.9 59.7 %copy-start.4 = (bf16[2048,256]{1,0:T(8,128)(2,1)S(1)}, bf16[2048,256]{1,0:T(8,128)(2,1)}, u32[]{:S(2)}) copy-start(bf16[2048,256]{1,0:T(8,128)(2,1)} %param.13) | copy-start | bytes 3145732
  136.9 61.8 %all-to-all-start.2 = ((bf16[16,16,2048]{2,1,0:T(8,128)(2,1)}), bf16[16,16,2048]{2,1,0:T(8,128)(2,1)S(1)}, u32[]{:S(2)}, u32[]{:S(2)}) async-start(bf16[16,16,2048]{2,1,0:T(8,128)(2,1)} %bitcast.20), calls=%async_computation.3 | async-start | bytes 2097152 | tf_op jit(solution)/shard_map/all_to_all | solution.py:57
  148.6 48.1 %reduce-scatter.7.cloned.1.call-start = ((), (), s32[]{:S(2)}) async-start(), calls=%async_computation.8 | async-start | bytes 163840 | tf_op jit(solution)/shard_map/reshape | solution.py:162
  196.6 13.2 %copy-start.8 = (bf16[64,256]{1,0:T(8,128)(2,1)S(1)}, bf16[64,256]{1,0:T(8,128)(2,1)}, u32[]{:S(2)}) copy-start(bf16[64,256]{1,0:T(8,128)(2,1)} %reduce-scatter.7.cloned.1.call-done) | copy-start | bytes 98308
  198.7 12.9 %copy-start.5 = (bf16[16,16,2048]{2,1,0:T(8,128)(2,1)}, bf16[16,16,2048]{2,1,0:T(8,128)(2,1)S(1)}, u32[]{:S(2)}) copy-start(bf16[16,16,2048]{2,1,0:T(8,128)(2,1)S(1)} %all-to-all-done.2) | copy-start | bytes 3145732
  198.7 21.3 %all-to-all-start.1 = ((bf16[16,4,2048]{2,1,0:T(4,128)(2,1)}), bf16[16,4,2048]{2,1,0:T(4,128)(2,1)S(1)}, u32[]{:S(2)}, u32[]{:S(2)}) async-start(bf16[16,4,2048]{2,1,0:T(4,128)(2,1)} %reshape.145), calls=%async_computation.2 | async-start | bytes 524288 | tf_op jit(solution)/shard_map/all_to_all | solution.py:57
  211.6 19.0 %copy-start.7 = (bf16[4,2048]{1,0:T(4,128)(2,1)S(1)}, bf16[4,2048]{1,0:T(4,128)(2,1)}, u32[]{:S(2)}) copy-start(bf16[4,2048]{1,0:T(4,128)(2,1)} %param.10) | copy-start | bytes 49156
  220.0 56.8 %all-to-all-start.3 = ((f32[32,64,256]{2,1,0:T(8,128)}), f32[32,64,256]{2,1,0:T(8,128)S(1)}, u32[]{:S(2)}, u32[]{:S(2)}) async-start(f32[32,64,256]{2,1,0:T(8,128)} %fusion.19), calls=%async_computation.4 | async-start | bytes 4194304 | tf_op jit(solution)/shard_map/all_to_all | solution.py:63
Sparse Core Ops, SparseCore 0:
  38.4 79.7 all-gather.1
  128.1 38.6 reduce-scatter.4
  170.2 26.3 reduce-scatter.6
where the time goes:
time: 287 us; the launch traced here: 284 us
  waiting for transfers between devices  148 us (52%)
  blocking collectives  53.9 us (19%)
  starting transfers between devices  29.8 us (10%)
  matrix products  22.3 us (8%)
  between operations  13.9 us (5%)
  other arithmetic  9.66 us (3%)
  local copies, waits for them, and re-layouts  6.56 us (2%)
    all_gather x1, waiting for transfers between devices, side_by_side(): whole = lax.all_gather(both, axis, axis=dim, tiled=True)  47.7 us
    all_to_all x1, waiting for transfers between devices, sum_at_owner_2(): parts = lax.all_to_all(cut_along(shard, dim, size), axis, 0, 0, tiled=True)  45.5 us
    all_to_all x1, blocking collectives, from_everyone(): return lax.all_to_all(copies, axis, split_axis=0, concat_axis=0, tiled=True)  31.5 us
    reshape x1, waiting for transfers between devices, body(): query_grad.astype(jnp.bfloat16).reshape(target_count, query_width)  28.1 us
    all_gather x1, blocking collectives, body(): lax.all_gather(jnp.stack([normed, output_grad]), 'tp', axis=1, tiled=True)  22.4 us
    all_to_all x2, starting transfers between devices, sum_at_owner(): parts = lax.all_to_all(cut_along(shard, dim, size), axis, 0, 0, tiled=True)  21.3 us
    reduce_scatter x1, waiting for transfers between devices, sum_by_axis(): nearer = lax.psum_scatter(shard, axes[0], scatter_dimension=dim, tiled=True)  18.2 us
    dot_general x4, matrix products, contract_last(): lax.dot_general(left, right, (((1,), (1,)), ((), ())), preferred_element_...  10.7 us
  transfers between devices with their start and end apart: 6, of which 5 were waited for; matrix products, arithmetic and copies ran while one was open for 7% of the time, Pallas kernels for 0%

commit v1 on v0

v1 whole, which is shorter than its diff:
```python
import math

import jax
import jax.numpy as jnp
from jax import lax
from jax.experimental import pallas as pl
from jax.experimental.pallas import tpu as pltpu
from jax.sharding import Mesh
from jax.sharding import PartitionSpec as P

SP = ("sp_0", "sp_1")
SP_TP = ("sp_0", "sp_1", "tp")
EPSILON = 1e-06
SCALE = 256 ** (-0.5)
SHIFT = math.log(8192)
MESH = pl.DeviceIdType.MESH
F32 = jnp.float32
BF16 = jnp.bfloat16
NZ, NX, NY = 8, 4, 8

SENDS, RECVS = 256, 256


def nt(left, right):
    return lax.dot_general(left, right, (((1,), (1,)), ((), ())), preferred_element_type=F32)


def nn(left, right):
    return lax.dot_general(left, right, (((1,), (0,)), ((), ())), preferred_element_type=F32)


def kernel(
    tr_ref, sr_ref, gain_ref, wq_hbm, wk_hbm, wv_hbm, wo_hbm, saved_ref, off_ref, og_ref,
    tgrad_ref, sgrad_ref, wgrad_ref,
    tg, xn, xo, xnt, sg, wq, wk, wv, wo, zf, xf, kb, vb, dk, dv,
    part1, reli1, relo1, xin1, zout1, zin1,
    part2, reli2, relo2, xin2, zout2, zin2,
    gout, gin, gsum, grecv, nout, nin, nsum, nrecv,
    ssem, rsem, wsem,
):
    z = lax.axis_index("sp_0")
    x = lax.axis_index("sp_1")
    t = lax.axis_index("tp")
    y = t // 2
    c = t % 2
    way = 1 - 2 * c

    def zat(k):
        return ((z + k) % NZ, x, t)

    def xat(k):
        return (z, (x + k) % NX, t)

    def yat(k):
        return (z, x, ((y + k) % NY) * 2 + c)

    mate = (z, x, t + way)
    ids = {"s": 0}
    names = {}
    pending = []

    def slot_of(name):
        if name not in names:
            names[name] = len(names)
        return names[name]

    def send(src, dst, name, dev):
        k = ids["s"]
        ids["s"] = k + 1
        copy = pltpu.make_async_remote_copy(
            src_ref=src, dst_ref=dst, send_sem=ssem.at[k], recv_sem=rsem.at[slot_of(name)],
            device_id=dev, device_id_type=MESH,
        )
        copy.start()
        pending.append(copy)

    def wait(dst, name):
        pltpu.make_async_remote_copy(
            src_ref=dst, dst_ref=dst, send_sem=ssem.at[0], recv_sem=rsem.at[slot_of(name)],
            device_id=mate, device_id_type=MESH,
        ).wait_recv()

    weights = {}
    for k, (name, src, dst) in enumerate(
        (("q", wq_hbm, wq), ("o", wo_hbm, wo), ("k", wk_hbm, wk), ("v", wv_hbm, wv))
    ):
        weights[name] = pltpu.make_async_copy(src, dst, wsem.at[k])
        weights[name].start()

    barrier = pltpu.get_barrier_semaphore()
    peers = [mate] + [yat(k) for k in range(1, NY)] + [xat(1), xat(3)] + [zat(k) for k in range(1, NZ)]
    for dev in peers:
        pl.semaphore_signal(barrier, inc=1, device_id=dev, device_id_type=MESH)

    gain = gain_ref[...].astype(F32)
    target = tr_ref[...].astype(F32)
    inverse = lax.rsqrt(jnp.mean(target * target, axis=1, keepdims=True) + EPSILON)
    tg[t] = jnp.concatenate(
        [target * inverse * gain, og_ref[...].astype(F32)], axis=0
    ).astype(BF16)
    sg[0] = sr_ref[...]
    pl.semaphore_wait(barrier, len(peers))

    def tg_of(k):
        return tg.at[((y + NY - k) % NY) * 2 + c]

    def tg_mate(k):
        return tg.at[((y + NY - k) % NY) * 2 + 1 - c]

    for k in (3, 5, 2, 6, 1, 7):
        send(tg_of(0), tg_of(0), ("tg", k), yat(k))
    send(tg_of(0), tg_of(0), ("tgm", 0), mate)
    for k in (3, 5, 2, 6, 1, 7):
        send(sr_ref, sg.at[k], ("sg", k), yat(k))
    send(sr_ref, sg.at[8], ("sgm", 0), mate)

    for k in (1, 7, 2, 6, 3, 5):
        wait(tg_of(k), ("tg", k))
        send(tg_of(k), tg_of(k), ("tgm", k), mate)
    relay = tg.at[((y + NY - 3 * way) % NY) * 2 + c]
    send(relay, relay, ("tg", 4), (z, x, ((y + NY + way) % NY) * 2 + c))
    wait(tg_of(4), ("tg", 4))
    send(tg_of(4), tg_of(4), ("tgm", 4), mate)
    for k in (0, 1, 7, 2, 6, 3, 5, 4):
        wait(tg_mate(k), ("tgm", k))

    for s in range(16):
        rows = tg[s].astype(F32)
        xn[4 * s : 4 * s + 4] = rows[0:4]
        xo[4 * s : 4 * s + 4] = rows[4:8]
    weights["q"].wait()
    queries = nn(xn[...].astype(BF16), wq[...]).astype(BF16)
    zf[0, x, 0:64] = queries
    weights["o"].wait()
    hgrad = nt(xo[...].astype(BF16), wo[...]).astype(BF16)
    xf[0, x] = hgrad
    deltas = jnp.sum(hgrad.astype(F32) * saved_ref[...].astype(F32), axis=1, keepdims=True)
    lane = lax.broadcasted_iota(jnp.int32, (64, 128), 1)
    both = jnp.where(lane == 0, off_ref[...].astype(F32), jnp.where(lane == 1, deltas, 0.0))
    place = lax.broadcasted_iota(jnp.int32, (64, 256), 1) == x * 64 + lax.broadcasted_iota(
        jnp.int32, (64, 256), 0
    )
    stats = nn(both.T.astype(BF16), place.astype(F32).astype(BF16))
    zf[0, x, 64:80] = stats[0:16].astype(BF16)

    def xs(e):
        return (x + NX - e) % NX

    def zf_x(k):
        send(zf.at[k, x], zf.at[k, x], ("zfx", k, 1), xat(1))
        send(zf.at[k, x], zf.at[k, x], ("zfx", k, 3), xat(3))

    def zf_z(k):
        if k:
            wait(zf.at[k, x], ("zfz", k))
        if k <= 3:
            send(zf.at[k, x], zf.at[k + 1, x], ("zfz", k + 1), zat(1))
        if k == 0 or k >= 6:
            send(zf.at[k, x], zf.at[(k - 1) % NZ, x], ("zfz", (k - 1) % NZ), zat(7))

    def zf_relay(k):
        wait(zf.at[k, xs(1)], ("zfx", k, 1))
        wait(zf.at[k, xs(3)], ("zfx", k, 3))
        e = 1 if k % 2 == 0 else 3
        send(zf.at[k, xs(e)], zf.at[k, xs(e)], ("zfx", k, 2), xat(e))

    def zf_end(k):
        wait(zf.at[k, xs(2)], ("zfx", k, 2))

    def xf_z(k, e):
        if k:
            wait(xf.at[k, xs(e)], ("xfz", k, e))
        if k <= 2:
            send(xf.at[k, xs(e)], xf.at[k + 1, xs(e)], ("xfz", k + 1, e), zat(1))
        if k == 0 or k >= 5:
            send(xf.at[k, xs(e)], xf.at[(k - 1) % NZ, xs(e)], ("xfz", (k - 1) % NZ, e), zat(7))

    def sg_in(k):
        wait(sg.at[k], ("sg", k))
        send(sg.at[k], sg.at[8 + k], ("sgm", k), mate)

    send(xf.at[0, x], xf.at[0, x], ("xfx", 1), xat(1))
    send(xf.at[0, x], xf.at[0, x], ("xfx", 3), xat(3))
    zf_z(0)
    xf_z(0, 0)
    zf_x(0)

    sg_in(1)
    sg_in(7)
    wait(xf.at[0, xs(1)], ("xfx", 1))
    xf_z(0, 1)
    wait(xf.at[0, xs(3)], ("xfx", 3))
    send(xf.at[0, xs(3)], xf.at[0, xs(3)], ("xfx", 2), xat(3))
    xf_z(0, 3)
    zf_z(1)
    zf_z(7)
    zf_x(1)
    zf_x(7)
    zf_relay(0)
    wait(xf.at[0, xs(2)], ("xfx", 2))
    xf_z(0, 2)
    sg_in(2)
    sg_in(6)
    for e in range(4):
        xf_z(1, e)
        xf_z(7, e)
    zf_z(2)
    zf_z(6)
    zf_x(2)
    zf_x(6)
    zf_relay(1)
    zf_relay(7)
    sg_in(3)
    sg_in(5)
    far = 3 + 2 * c
    send(sg.at[far], sg.at[4], ("sg", 4), (z, x, ((y + NY + way) % NY) * 2 + c))
    for f in range(4):
        xnt[2 * f] = jnp.transpose(xn[:, 512 * f : 512 * f + 256]).astype(BF16)
        xnt[2 * f + 1] = jnp.transpose(xn[:, 512 * f + 256 : 512 * f + 512]).astype(BF16)
    for e in range(4):
        xf_z(2, e)
        xf_z(6, e)
    zf_z(3)
    zf_z(5)
    zf_x(3)
    zf_x(5)
    zf_relay(2)
    zf_relay(6)
    sg_in(4)
    for e in range(4):
        xf_z(3, e)
        xf_z(5, e)
    zf_z(4)
    zf_x(4)
    zf_relay(3)
    zf_relay(5)
    for k in range(8):
        wait(sg.at[8 + k], ("sgm", k))
    rows = sg[...].reshape(256, 2048)
    weights["k"].wait()
    kb[...] = nn(rows, wk[...]).astype(BF16)
    zf_relay(4)
    weights["v"].wait()
    vb[...] = nn(rows, wv[...]).astype(BF16)

    def x_sends(tag, k, part, reli, xin):
        e = 1 if k % 2 == 0 else 3
        send(part.at[k, (x + 2) % NX], reli.at[k], (tag, "rel", k), xat(e))
        send(part.at[k, (x + 4 - e) % NX], xin.at[k, 1], (tag, "x1", k), xat(4 - e))

    def x_relay(tag, k, part, reli, relo, xin):
        e = 1 if k % 2 == 0 else 3
        wait(reli.at[k], (tag, "rel", k))
        relo[k] = (part[k, (x + e) % NX].astype(F32) + reli[k].astype(F32)).astype(BF16)
        send(relo.at[k], xin.at[k, 0], (tag, "x0", k), xat(e))

    def x_sum(tag, k, part, xin):
        wait(xin.at[k, 0], (tag, "x0", k))
        wait(xin.at[k, 1], (tag, "x1", k))
        return part[k, x].astype(F32) + xin[k, 0].astype(F32) + xin[k, 1].astype(F32)

    def z_send(tag, k, part, xin, zout, zin):
        zout[k] = x_sum(tag, k, part, xin).astype(BF16)
        send(zout.at[k], zin.at[k], (tag, "z", k), zat(NZ - k))

    def z_sum(tag, part, xin, zin):
        total = x_sum(tag, 0, part, xin)
        for k in range(1, NZ):
            wait(zin.at[k], (tag, "z", k))
            total += zin[k].astype(F32)
        return total

    def group(k, first):
        q = zf[k, :, 0:64, :].reshape(256, 256)
        h = xf[k].reshape(256, 256)
        stat = jnp.sum(zf[k, :, 64:80, :].astype(F32), axis=0)
        score = nt(kb[...], q)
        prob = jnp.exp(score * SCALE - (SHIFT + stat[0:1]))
        grad = prob * (nt(vb[...], h) - stat[1:2]) * SCALE
        prob = prob.astype(BF16)
        dv_new = nn(prob, h)
        dk_new = nn(grad.astype(BF16), q)
        if first:
            dv[...] = dv_new
            dk[...] = dk_new
        else:
            dv[...] += dv_new
            dk[...] += dk_new
        dq = nn(jnp.transpose(grad).astype(BF16), kb[...])
        part1[k] = dq.astype(BF16).reshape(4, 64, 256)

    for e in range(4):
        xf_z(4, e)
    order = (1, 7, 2, 6, 3, 5, 4, 0)
    one = (part1, reli1)
    for n, k in enumerate(order):
        zf_end(k)
        group(k, n == 0)
        x_sends("q", k, part1, reli1, xin1)
        if n >= 1:
            x_relay("q", order[n - 1], part1, reli1, relo1, xin1)
        if n >= 2:
            z_send("q", order[n - 2], part1, xin1, zout1, zin1)
    x_relay("q", 0, part1, reli1, relo1, xin1)
    z_send("q", 4, part1, xin1, zout1, zin1)

    dkb = dk[...].astype(BF16)
    dvb = dv[...].astype(BF16)
    for half in (1, 0):
        for f in range(4):
            cols = pl.ds(512 * f, 512)
            lo = 128 * half
            gout[half, :, :, cols] = (
                (nt(dkb[lo : lo + 128], wk[cols, :]) + nt(dvb[lo : lo + 128], wv[cols, :]))
                .astype(BF16)
                .reshape(8, 16, 512)
            )
        if half:
            send(gout.at[1], gin, ("gm",), mate)
    wait(gin, ("gm",))
    for k in (4, 3, 5, 2, 6, 1, 7):
        gsum[k] = (gout[0, k].astype(F32) + gin[k].astype(F32)).astype(BF16)
        send(gsum.at[k], grecv.at[k], ("g", k), yat(NY - k))

    qflat = z_sum("q", part1, xin1, zin1).astype(BF16)

    def weight_part(k):
        part2[k] = nn(xnt[(z + NZ - k) % NZ], qflat).astype(BF16).reshape(4, 64, 256)

    for n, k in enumerate(order):
        weight_part(k)
        x_sends("w", k, part2, reli2, xin2)
        if n >= 2:
            x_relay("w", order[n - 2], part2, reli2, relo2, xin2)

    for f in range(2):
        halves = [nt(qflat, wq[1024 * g + 512 * f : 1024 * g + 512 * f + 512, :]) for g in range(2)]
        for s in range(16):
            nout[s % 2, s // 2, :, 512 * f : 512 * f + 512] = jnp.concatenate(
                [part[4 * s : 4 * s + 4] for part in halves], axis=0
            ).astype(BF16)
    send(nout.at[1 - c], nin, ("nm",), mate)
    x_relay("w", 4, part2, reli2, relo2, xin2)
    x_relay("w", 0, part2, reli2, relo2, xin2)
    wait(nin, ("nm",))
    nsum[...] = (nout[c].astype(F32) + nin[...].astype(F32)).astype(BF16)
    for k in (4, 3, 5, 2, 6, 1, 7):
        send(nsum.at[(y + NY - k) % NY], nrecv.at[k], ("n", k), yat(NY - k))
    for k in order[:-1]:
        z_send("w", k, part2, xin2, zout2, zin2)

    total = gout[0, 0].astype(F32) + gin[0].astype(F32)
    for k in (1, 7, 2, 6, 3, 5, 4):
        wait(grecv.at[k], ("g", k))
        total += grecv[k].astype(F32)
    sgrad_ref[...] = total

    total = nsum[y].astype(F32)
    for k in (1, 7, 2, 6, 3, 5, 4):
        wait(nrecv.at[k], ("n", k))
        total += nrecv[k].astype(F32)
    scaled = jnp.concatenate([total[0:4], total[4:8]], axis=1) * gain
    mean = jnp.mean(scaled * target, axis=1, keepdims=True)
    tgrad_ref[...] = inverse * scaled - target * (inverse * inverse * inverse) * mean

    wgrad_ref[...] = z_sum("w", part2, xin2, zin2)

    for copy in pending:
        copy.wait_send()
    assert ids["s"] <= SENDS and len(names) <= RECVS


def body(tr, sr, gain, wq, wk, wv, wo, saved, offset, og):
    vm = pl.BlockSpec(memory_space=pltpu.VMEM)
    hb = pl.BlockSpec(memory_space=pl.ANY)

    def buf(*shape, dtype=BF16):
        return pltpu.VMEM(shape, dtype)

    reduce_bufs = [
        buf(8, 4, 64, 256), buf(8, 64, 256), buf(8, 64, 256), buf(8, 2, 64, 256),
        buf(8, 64, 256), buf(8, 64, 256),
    ]
    return pl.pallas_call(
        kernel,
        out_shape=(
            jax.ShapeDtypeStruct((4, 2048), F32),
            jax.ShapeDtypeStruct((16, 2048), F32),
            jax.ShapeDtypeStruct((64, 256), F32),
        ),
        in_specs=[vm, vm, vm, hb, hb, hb, hb, vm, vm, vm],
        out_specs=(vm, vm, vm),
        scratch_shapes=[
            buf(16, 8, 2048), buf(64, 2048, dtype=F32), buf(64, 2048, dtype=F32),
            buf(8, 256, 64), buf(16, 16, 2048),
            buf(2048, 256), buf(2048, 256), buf(2048, 256), buf(256, 2048),
            buf(8, 4, 80, 256), buf(8, 4, 64, 256),
            buf(256, 256), buf(256, 256),
            buf(256, 256, dtype=F32), buf(256, 256, dtype=F32),
            *reduce_bufs, *reduce_bufs,
            buf(2, 8, 16, 2048), buf(8, 16, 2048), buf(8, 16, 2048), buf(8, 16, 2048),
            buf(2, 8, 8, 1024), buf(8, 8, 1024), buf(8, 8, 1024), buf(8, 8, 1024),
            pltpu.SemaphoreType.DMA((SENDS,)),
            pltpu.SemaphoreType.DMA((RECVS,)),
            pltpu.SemaphoreType.DMA((4,)),
        ],
        compiler_params=pltpu.CompilerParams(
            collective_id=0, has_side_effects=True, vmem_limit_bytes=60 * 1024 * 1024
        ),
    )(tr, sr, gain.reshape(1, 2048), wq, wk, wv, wo, saved, offset, og)


def solution(mesh):
    split = Mesh(mesh.devices.reshape(NZ, NX, mesh.shape["tp"]), ("sp_0", "sp_1", "tp"))
    placed = (
        P(SP_TP, None), P(SP_TP, None), P(), P(None, "tp"), P(None, "tp"), P(None, "tp"),
        P("tp", None), P(SP, "tp"), P(SP, "tp"), P(SP_TP, None),
    )
    return jax.shard_map(
        body,
        mesh=split,
        in_specs=placed,
        out_specs=(P(SP_TP, None), P(SP_TP, None), P(SP, "tp")),
        check_vma=False,
    )
```

time: 287 us -> 111 us (0.39)
  the two profiles are of different devices: /device:TPU:1 before, /device:TPU:7 now
where the time goes in v1:
time: 111 us
  Pallas kernels  105 us (95%)
  local copies, waits for them, and re-layouts  5.62 us (5%)
    pallas_call x1, Pallas kernels, body(): pl.pallas_call(kernel, out_shape=(jax.ShapeDtypeStruct((4, 2048), F32), j...  105 us
    unnamed x8, local copies, waits for them, and re-layouts  4.32 us

profile of v1, /device:TPU:7, one launch (start us, length us, event | category | flops | bytes accessed | tf_op | source)
XLA Modules:
  0.0 111.0 jit_solution(18349415841798242686)
XLA Ops:
  0.6 0.0 copy-start.1
  0.6 1.3 %reshape.9.gain_ref = bf16[1,2048]{1,0:T(2,128)(2,1)} reshape(bf16[2048]{0:T(1024)(128)(2,1)} %param.12) | data formatting | bytes 8192 | tf_op jit(solution)/shard_map/reshape | solution.py:410
  1.9 0.0 copy-done.1
  1.9 0.7 copy.13.off_ref
  2.6 104.8 %shard_map.121 = (f32[4,2048]{1,0:T(4,128)}, f32[16,2048]{1,0:T(8,128)}, f32[64,256]{1,0:T(8,128)}) custom-call(bf16[4,2048]{1,0:T(4,128)(2,1)} %tr_ref.1, bf16[16,2048]{1,0:T(8,128)(2,1)} %sr_ref.1, bf16[1,2048]{1,0:T(2,128)(2,1)} %reshape.9.gain_ref, bf16[2048,256]{1,0:T(8,128)(2,1)} %wq_hbm.1, bf16[2048,256]{1,0:T(8,128)(2,1)} %wk_hbm.1, ...), custom_call_target="tpu_custom_call" | custom-call | tf_op jit(solution)/shard_map/pallas_call | solution.py:384
  107.4 1.4 %copy.17 = f32[4,2048]{1,0:T(4,128)} copy(f32[4,2048]{1,0:T(4,128)} %get-tuple-element.6) | data formatting | bytes 65536
  108.8 0.0 copy-start
  108.8 1.6 %copy.18 = f32[16,2048]{1,0:T(8,128)} copy(f32[16,2048]{1,0:T(8,128)} %get-tuple-element.7) | data formatting | bytes 262144
  110.4 0.0 copy-done
  110.4 0.6 copy.19
Async XLA Ops:
  0.6 1.3 %copy-start.1 = (bf16[64,1]{0,1:T(2,128)(2,1)S(1)}, bf16[64,1]{0,1:T(2,128)(2,1)}, u32[]{:S(2)}) copy-start(bf16[64,1]{0,1:T(2,128)(2,1)} %param.18) | copy-start | bytes 388
  108.8 1.6 %copy-start = (f32[64,256]{1,0:T(8,128)S(1)}, f32[64,256]{1,0:T(8,128)}, u32[]{:S(2)}) copy-start(f32[64,256]{1,0:T(8,128)} %get-tuple-element.8) | copy-start | bytes 196612

commit v2 on v1

v2 whole, which is shorter than its diff:
```python
import math

import jax
import jax.numpy as jnp
from jax import lax
from jax.experimental import pallas as pl
from jax.experimental.pallas import tpu as pltpu
from jax.sharding import Mesh
from jax.sharding import PartitionSpec as P

SP = ("sp_0", "sp_1")
SP_TP = ("sp_0", "sp_1", "tp")
EPSILON = 1e-06
SCALE = 256 ** (-0.5)
SHIFT = math.log(8192)
MESH = pl.DeviceIdType.MESH
F32 = jnp.float32
BF16 = jnp.bfloat16
NZ, NX, NY = 8, 4, 8
UNIT = 8192
UNITS = 1024
RECVS = 112


def nt(left, right):
    return lax.dot_general(left, right, (((1,), (1,)), ((), ())), preferred_element_type=F32)


def nn(left, right):
    return lax.dot_general(left, right, (((1,), (0,)), ((), ())), preferred_element_type=F32)


def kernel(
    tr_hbm, sr_hbm, gain_hbm, wq_hbm, wk_hbm, wv_hbm, wo_hbm, saved_hbm, off_hbm, og_hbm,
    tgrad_ref, sgrad_ref, wgrad_ref,
    tr, gn, sv, of, og,
    tg, xn, xo, nb, nr, nrt, sg, wq, wk, wv, wo, zf, xf, kb, vb, dk, dv,
    part, reli, relo, xin, zout, zin,
    qz, wpart, win,
    gout, gin, gsum, grecv, nout, nin, nsum, nrecv,
    units, ssem, rsem, lsem,
):
    z = lax.axis_index("sp_0")
    x = lax.axis_index("sp_1")
    t = lax.axis_index("tp")
    y = t // 2
    c = t % 2
    way = 1 - 2 * c

    def zat(k):
        return ((z + k) % NZ, x, t)

    def xat(k):
        return (z, (x + k) % NX, t)

    def yat(k):
        return (z, x, ((y + k) % NY) * 2 + c)

    mate = (z, x, t + way)
    names = {}
    sent = [0]
    scope = [None]

    def phase(name):
        if scope[0] is not None:
            scope[0].__exit__(None, None, None)
        scope[0] = jax.named_scope(name) if name else None
        if name:
            scope[0].__enter__()

    def size(ref):
        return math.prod(ref.shape) * 2

    def slot_of(name):
        if name not in names:
            names[name] = len(names)
        return names[name]

    def send(src, dst, name, dev):
        assert size(src) % UNIT == 0
        sent[0] += size(src) // UNIT
        pltpu.make_async_remote_copy(
            src_ref=src, dst_ref=dst, send_sem=ssem.at[0], recv_sem=rsem.at[slot_of(name)],
            device_id=dev, device_id_type=MESH,
        ).start()

    def wait(dst, name):
        pltpu.make_async_remote_copy(
            src_ref=dst, dst_ref=dst, send_sem=ssem.at[0], recv_sem=rsem.at[slot_of(name)],
            device_id=mate, device_id_type=MESH,
        ).wait_recv()

    phase("start")
    loads = {}
    for k, (name, src, dst) in enumerate(
        (
            ("tr", tr_hbm, tr), ("og", og_hbm, og), ("gn", gain_hbm, gn), ("sr", sr_hbm, sg.at[0]),
            ("of", off_hbm, of), ("sv", saved_hbm, sv),
            ("q", wq_hbm, wq), ("o", wo_hbm, wo), ("k", wk_hbm, wk), ("v", wv_hbm, wv),
        )
    ):
        loads[name] = pltpu.make_async_copy(src, dst, lsem.at[k])
        loads[name].start()

    barrier = pltpu.get_barrier_semaphore()
    peers = [mate] + [yat(k) for k in range(1, NY)] + [xat(k) for k in range(1, NX)]
    peers += [zat(k) for k in range(1, NZ)]
    for dev in peers:
        pl.semaphore_signal(barrier, inc=1, device_id=dev, device_id_type=MESH)

    for name in ("tr", "og", "gn"):
        loads[name].wait()
    gain = gn[...].astype(F32)
    gain = jnp.concatenate([gain[s : s + 1] for s in range(16)], axis=1)
    target = tr[...].astype(F32)
    inverse = lax.rsqrt(jnp.mean(target * target, axis=1, keepdims=True) + EPSILON)
    tg[c, y] = jnp.concatenate(
        [target * inverse * gain, og[...].astype(F32)], axis=0
    ).astype(BF16)
    phase("barrier")
    pl.semaphore_wait(barrier, len(peers))

    phase("tgwait")

    def tg_of(k):
        return tg.at[c, (y + NY - k) % NY]

    for k in (4, 3, 5, 2, 6, 1, 7):
        send(tg_of(0), tg_of(0), ("tg", k), yat(k))
    send(tg_of(0), tg_of(0), ("tgm",), mate)
    for k in (1, 7, 2, 6, 3, 5, 4):
        wait(tg_of(k), ("tg", k))
        send(tg_of(k), tg_of(k), ("tgm",), mate)
    loads["sr"].wait()
    for k in (3, 5, 2, 6, 1, 7):
        send(sg.at[0], sg.at[k], ("sg", k), yat(k))
    send(sg.at[0], sg.at[8], ("sgm",), mate)
    phase("tgmate")
    wait(tg.at[1 - c], ("tgm",))

    phase("qproj")
    for s in range(16):
        rows = tg[s % 2, s // 2].astype(F32)
        xn[4 * s : 4 * s + 4] = rows[0:4]
        xo[4 * s : 4 * s + 4] = rows[4:8]
    loads["q"].wait()
    queries = nn(xn[...].astype(BF16), wq[...]).astype(BF16)
    zf[0, x, 0:64] = queries
    loads["o"].wait()
    hgrad = nt(xo[...].astype(BF16), wo[...]).astype(BF16)
    xf[0, x] = hgrad
    loads["sv"].wait()
    loads["of"].wait()
    deltas = jnp.sum(hgrad.astype(F32) * sv[...].astype(F32), axis=1, keepdims=True)
    deltas = jnp.broadcast_to(deltas, (64, 128)).T[0:16]
    first = lax.broadcasted_iota(jnp.int32, (16, 64), 0) == 0
    both = jnp.where(first, of[...].astype(F32), deltas).astype(BF16)
    place = lax.broadcasted_iota(jnp.int32, (64, 256), 1) == x * 64 + lax.broadcasted_iota(
        jnp.int32, (64, 256), 0
    )
    zf[0, x, 64:80] = nn(both, place.astype(F32).astype(BF16)).astype(BF16)

    def xs(e):
        return (x + NX - e) % NX

    def zf_x(k):
        send(zf.at[k, x], zf.at[k, x], ("zfx", k, 1), xat(1))
        send(zf.at[k, x], zf.at[k, x], ("zfx", k, 3), xat(3))

    def zf_z(k):
        if k:
            wait(zf.at[k, x], ("zfz", k))
        if k <= 3:
            send(zf.at[k, x], zf.at[k + 1, x], ("zfz", k + 1), zat(1))
        if k == 0 or k >= 6:
            send(zf.at[k, x], zf.at[(k - 1) % NZ, x], ("zfz", (k - 1) % NZ), zat(7))

    def zf_relay(k):
        wait(zf.at[k, xs(1)], ("zfx", k, 1))
        wait(zf.at[k, xs(3)], ("zfx", k, 3))
        e = 1 if k % 2 == 0 else 3
        send(zf.at[k, xs(e)], zf.at[k, xs(e)], ("zfx", k, 2), xat(e))

    def zf_end(k):
        wait(zf.at[k, xs(2)], ("zfx", k, 2))

    def xf_z(k, e):
        if k:
            wait(xf.at[k, xs(e)], ("xfz", k, e))
        if k <= 2:
            send(xf.at[k, xs(e)], xf.at[k + 1, xs(e)], ("xfz", k + 1, e), zat(1))
        if k == 0 or k >= 5:
            send(xf.at[k, xs(e)], xf.at[(k - 1) % NZ, xs(e)], ("xfz", (k - 1) % NZ, e), zat(7))

    def sg_in(k):
        wait(sg.at[k], ("sg", k))
        send(sg.at[k], sg.at[8 + k], ("sgm",), mate)

    phase("spsend")
    send(xf.at[0, x], xf.at[0, x], ("xfx", 1), xat(1))
    send(xf.at[0, x], xf.at[0, x], ("xfx", 3), xat(3))
    zf_z(0)
    xf_z(0, 0)
    zf_x(0)

    phase("step1")
    for f in range(8):
        nb[f] = xn[:, 256 * f : 256 * f + 256].astype(BF16)
    wait(xf.at[0, xs(1)], ("xfx", 1))
    xf_z(0, 1)
    wait(xf.at[0, xs(3)], ("xfx", 3))
    send(xf.at[0, xs(3)], xf.at[0, xs(3)], ("xfx", 2), xat(3))
    xf_z(0, 3)
    zf_z(1)
    zf_z(7)
    zf_x(1)
    zf_x(7)
    zf_relay(0)
    sg_in(1)
    sg_in(7)
    wait(xf.at[0, xs(2)], ("xfx", 2))
    xf_z(0, 2)
    phase("step2")
    for e in (0, 1, 3, 2):
        xf_z(1, e)
        xf_z(7, e)
    zf_z(2)
    zf_z(6)
    zf_x(2)
    zf_x(6)
    sg_in(2)
    sg_in(6)
    zf_relay(1)
    zf_relay(7)
    phase("step3")
    for e in (0, 1, 3, 2):
        xf_z(2, e)
        xf_z(6, e)
    sg_in(3)
    sg_in(5)
    send(sg.at[3 + 2 * c], sg.at[4], ("sg", 4), (z, x, ((y + NY + way) % NY) * 2 + c))
    zf_z(3)
    zf_z(5)
    zf_x(3)
    zf_x(5)
    zf_relay(2)
    zf_relay(6)
    sg_in(4)
    phase("step4")
    for e in (0, 1, 3, 2):
        xf_z(3, e)
        xf_z(5, e)
    zf_z(4)
    zf_x(4)
    for k in range(1, NZ):
        send(nb.at[(z + k) % NZ], nr.at[k], ("nb",), zat(k))
    phase("kproj")
    wait(sg.at[8:16], ("sgm",))
    loads["k"].wait()
    kb[...] = nn(sg[...].reshape(256, 2048), wk[...]).astype(BF16)
    zf_relay(3)
    zf_relay(5)
    phase("vproj")
    loads["v"].wait()
    vb[...] = nn(sg[...].reshape(256, 2048), wv[...]).astype(BF16)
    zf_relay(4)

    def x_sends(k):
        e = 1 if k % 2 == 0 else 3
        send(part.at[k, (x + 2) % NX], reli.at[k], ("rel", k), xat(e))
        send(part.at[k, (x + 4 - e) % NX], xin.at[k, 1], ("xin", k), xat(4 - e))

    def x_relay(k):
        e = 1 if k % 2 == 0 else 3
        wait(reli.at[k], ("rel", k))
        relo[k] = (part[k, (x + e) % NX].astype(F32) + reli[k].astype(F32)).astype(BF16)
        send(relo.at[k], xin.at[k, 0], ("xin", k), xat(e))

    def x_sum(k):
        wait(xin.at[k], ("xin", k))
        return part[k, x].astype(F32) + xin[k, 0].astype(F32) + xin[k, 1].astype(F32)

    def z_send(k):
        if k:
            zout[k] = x_sum(k).astype(BF16)
            send(zout.at[k], zin.at[k], ("zin",), zat(NZ - k))

    def group(k, first):
        q = zf[k, :, 0:64, :].reshape(256, 256)
        h = xf[k].reshape(256, 256)
        stat = jnp.sum(zf[k, :, 64:80, :].astype(F32), axis=0)
        score = nt(kb[...], q)
        prob = jnp.exp(score * SCALE - (SHIFT + stat[0:1]))
        grad = prob * (nt(vb[...], h) - stat[1:2]) * SCALE
        prob = prob.astype(BF16)
        dv_new = nn(prob, h)
        dk_new = nn(grad.astype(BF16), q)
        if first:
            dv[...] = dv_new
            dk[...] = dk_new
        else:
            dv[...] += dv_new
            dk[...] += dk_new
        dq = nn(jnp.transpose(grad).astype(BF16), kb[...])
        part[k] = dq.astype(BF16).reshape(4, 64, 256)

    order = (1, 7, 2, 6, 0, 3, 5, 4)
    for n, k in enumerate(order):
        phase(f"group{n}")
        if k == 3:
            for e in range(4):
                xf_z(4, e)
        zf_end(k)
        group(k, n == 0)
        x_sends(k)
        if n >= 3:
            phase(f"relay{n - 3}")
            x_relay(order[n - 3])
        if n >= 6:
            phase(f"zsend{n - 6}")
            z_send(order[n - 6])

    phase("gmat1")
    dkb = dk[...].astype(BF16)
    dvb = dv[...].astype(BF16)

    def gmat(half):
        lo = 128 * half
        for f in range(4):
            cols = pl.ds(512 * f, 512)
            gout[half, :, :, cols] = (
                (nt(dkb[lo : lo + 128], wk[cols, :]) + nt(dvb[lo : lo + 128], wv[cols, :]))
                .astype(BF16)
                .reshape(8, 16, 512)
            )

    gmat(1)
    send(gout.at[1], gin, ("gm",), mate)
    phase("relay5")
    x_relay(order[5])
    z_send(order[2])
    z_send(order[3])
    phase("relay6")
    x_relay(order[6])
    phase("gmat0")
    gmat(0)
    phase("relay7")
    x_relay(order[7])
    z_send(order[5])
    phase("nrt")
    nr[0] = nb[z]
    wait(nr.at[1:8], ("nb",))
    for j in range(4):
        pair = nr[2 * j : 2 * j + 2].reshape(128, 256).astype(F32)
        nrt[:, 128 * j : 128 * j + 128] = pair.T.astype(BF16)
    phase("zsend")
    z_send(order[6])
    z_send(order[7])
    phase("gsum")
    wait(gin, ("gm",))
    for k in (4, 3, 5, 2, 6, 1, 7):
        gsum[k] = (gout[0, k].astype(F32) + gin[k].astype(F32)).astype(BF16)
        send(gsum.at[k], grecv.at[k], ("g",), yat(NY - k))

    phase("qflat")
    total = x_sum(0)
    wait(zin.at[1:8], ("zin",))
    for k in range(1, NZ):
        total += zin[k].astype(F32)
    qflat = total.astype(BF16)
    qz[0] = qflat
    for k in (4, 3, 5, 2, 6, 1, 7):
        send(qz.at[0], qz.at[k], ("qz",), zat(k))

    phase("ng")
    for f in range(2):
        halves = [nt(qflat, wq[1024 * g + 512 * f : 1024 * g + 512 * f + 512, :]) for g in range(2)]
        for s in range(16):
            nout[s % 2, s // 2, :, 512 * f : 512 * f + 512] = jnp.concatenate(
                [half[4 * s : 4 * s + 4] for half in halves], axis=0
            ).astype(BF16)
    send(nout.at[1 - c], nin, ("nm",), mate)
    phase("nsum")
    wait(nin, ("nm",))
    nsum[...] = (nout[c].astype(F32) + nin[...].astype(F32)).astype(BF16)
    for k in (4, 3, 5, 2, 6, 1, 7):
        send(nsum.at[(y + NY - k) % NY], nrecv.at[k], ("n",), yat(NY - k))

    phase("wmat")
    wait(qz.at[1:8], ("qz",))
    wsum = nn(nrt[...], qz[...].reshape(512, 256))
    wpart[...] = wsum.astype(BF16).reshape(4, 64, 256)
    for e in (2, 1, 3):
        send(wpart.at[(x + e) % NX], win.at[e], ("w",), xat(e))

    phase("gfin")
    wait(grecv.at[1:8], ("g",))
    total = gout[0, 0].astype(F32) + gin[0].astype(F32)
    for k in range(1, NY):
        total += grecv[k].astype(F32)
    sgrad_ref[...] = total

    phase("nfin")
    wait(nrecv.at[1:8], ("n",))
    total = nsum[y].astype(F32)
    for k in range(1, NY):
        total += nrecv[k].astype(F32)
    scaled = jnp.concatenate([total[0:4], total[4:8]], axis=1) * gain
    mean = jnp.mean(scaled * target, axis=1, keepdims=True)
    tgrad_ref[...] = inverse * scaled - target * (inverse * inverse * inverse) * mean

    phase("wfin")
    wait(win.at[1:4], ("w",))
    total = wpart[x].astype(F32)
    for e in range(1, NX):
        total += win[e].astype(F32)
    wgrad_ref[...] = total

    phase("sendwait")
    all_sent = units.at[0 : sent[0]]
    pltpu.make_async_remote_copy(
        src_ref=all_sent, dst_ref=all_sent, send_sem=ssem.at[0], recv_sem=rsem.at[0],
        device_id=mate, device_id_type=MESH,
    ).wait_send()
    phase(None)
    assert sent[0] <= UNITS and len(names) <= RECVS, (sent[0], len(names))


def finish(a_ref, b_ref, c_ref, oa_ref, ob_ref, oc_ref):
    oa_ref[...] = a_ref[...]
    ob_ref[...] = b_ref[...]
    oc_ref[...] = c_ref[...]


def body(tr, sr, gain, wq, wk, wv, wo, saved, offset, og):
    vm = pl.BlockSpec(memory_space=pltpu.VMEM)
    hb = pl.BlockSpec(memory_space=pl.ANY)

    def buf(*shape, dtype=BF16):
        return pltpu.VMEM(shape, dtype)

    outs = (
        jax.ShapeDtypeStruct((4, 2048), F32),
        jax.ShapeDtypeStruct((16, 2048), F32),
        jax.ShapeDtypeStruct((64, 256), F32),
    )
    results = pl.pallas_call(
        kernel,
        out_shape=outs,
        in_specs=[hb] * 10,
        out_specs=(vm, vm, vm),
        scratch_shapes=[
            buf(4, 2048), buf(16, 128), buf(64, 256), buf(1, 64), buf(4, 2048),
            buf(2, 8, 8, 2048), buf(64, 2048, dtype=F32), buf(64, 2048, dtype=F32),
            buf(8, 64, 256), buf(8, 64, 256), buf(256, 512), buf(16, 16, 2048),
            buf(2048, 256), buf(2048, 256), buf(2048, 256), buf(256, 2048),
            buf(8, 4, 80, 256), buf(8, 4, 64, 256),
            buf(256, 256), buf(256, 256),
            buf(256, 256, dtype=F32), buf(256, 256, dtype=F32),
            buf(8, 4, 64, 256), buf(8, 64, 256), buf(8, 64, 256), buf(8, 2, 64, 256),
            buf(8, 64, 256), buf(8, 64, 256),
            buf(8, 64, 256), buf(4, 64, 256), buf(4, 64, 256),
            buf(2, 8, 16, 2048), buf(8, 16, 2048), buf(8, 16, 2048), buf(8, 16, 2048),
            buf(2, 8, 8, 1024), buf(8, 8, 1024), buf(8, 8, 1024), buf(8, 8, 1024),
            buf(UNITS, 16, 256),
            pltpu.SemaphoreType.DMA((1,)),
            pltpu.SemaphoreType.DMA((RECVS,)),
            pltpu.SemaphoreType.DMA((10,)),
        ],
        compiler_params=pltpu.CompilerParams(
            collective_id=0, has_side_effects=True, vmem_limit_bytes=60 * 1024 * 1024
        ),
    )(tr, sr, gain.reshape(16, 128), wq, wk, wv, wo, saved, offset.reshape(1, 64), og)
    return pl.pallas_call(
        finish, out_shape=outs, in_specs=[vm, vm, vm], out_specs=(vm, vm, vm)
    )(*results)


def solution(mesh):
    split = Mesh(mesh.devices.reshape(NZ, NX, mesh.shape["tp"]), ("sp_0", "sp_1", "tp"))
    placed = (
        P(SP_TP, None), P(SP_TP, None), P(), P(None, "tp"), P(None, "tp"), P(None, "tp"),
        P("tp", None), P(SP, "tp"), P(SP, "tp"), P(SP_TP, None),
    )
    return jax.shard_map(
        body,
        mesh=split,
        in_specs=placed,
        out_specs=(P(SP_TP, None), P(SP_TP, None), P(SP, "tp")),
        check_vma=False,
    )
```

time: 111 us -> 81.9 us (0.74)
  the two profiles are of different devices: /device:TPU:7 before, /device:TPU:2 now
where the time goes in v2:
time: 81.9 us; the launch traced here: 81.7 us
  Pallas kernels  81.1 us (99%)
    pallas_call x1, Pallas kernels, body(): pl.pallas_call(kernel, out_shape=outs, in_specs=[hb] * 10, out_specs=(vm,...  79.5 us

profile of v2, /device:TPU:2, one launch (start us, length us, event | category | flops | bytes accessed | tf_op | source)
XLA Modules:
  0.0 81.7 jit_solution(9203931848727111695)
XLA Ops:
  0.6 79.5 %shard_map.121 = (f32[4,2048]{1,0:T(4,128)}, f32[16,2048]{1,0:T(8,128)}, f32[64,256]{1,0:T(8,128)}) custom-call(bf16[4,2048]{1,0:T(4,128)(2,1)} %tr_hbm.1, bf16[16,2048]{1,0:T(8,128)(2,1)} %sr_hbm.1, bf16[16,128]{1,0:T(8,128)(2,1)} %bitcast.2, bf16[2048,256]{1,0:T(8,128)(2,1)} %wq_hbm.1, bf16[2048,256]{1,0:T(8,128)(2,1)} %wk_hbm.1, ...), custom_call_target="tpu_custom_call" | custom-call | tf_op jit(solution)/shard_map/pallas_call | solution.py:447
  80.1 1.6 %shard_map.122 = (f32[4,2048]{1,0:T(4,128)}, f32[16,2048]{1,0:T(8,128)}, f32[64,256]{1,0:T(8,128)}) custom-call(f32[4,2048]{1,0:T(4,128)} %get-tuple-element.6.a_ref, f32[16,2048]{1,0:T(8,128)} %get-tuple-element.7.b_ref, f32[64,256]{1,0:T(8,128)} %get-tuple-element.8.c_ref), custom_call_target="tpu_custom_call" | custom-call | tf_op jit(solution)/shard_map/pallas_call | solution.py:474

commit v3 on v2

--- a/solution.py
+++ b/solution.py
@@ -35,7 +35,7 @@
     tgrad_ref, sgrad_ref, wgrad_ref,
     tr, gn, sv, of, og,
     tg, xn, xo, nb, nr, nrt, sg, wq, wk, wv, wo, zf, xf, kb, vb, dk, dv,
-    part, reli, relo, xin, zout, zin,
+    part, near, reli, relo, xin, zout, zin,
     qz, wpart, win,
     gout, gin, gsum, grecv, nout, nin, nsum, nrecv,
     units, ssem, rsem, lsem,
@@ -76,9 +76,9 @@
             names[name] = len(names)
         return names[name]
 
-    def send(src, dst, name, dev):
+    def send(src, dst, name, dev, count=True):
         assert size(src) % UNIT == 0
-        sent[0] += size(src) // UNIT
+        sent[0] += count * size(src) // UNIT
         pltpu.make_async_remote_copy(
             src_ref=src, dst_ref=dst, send_sem=ssem.at[0], recv_sem=rsem.at[slot_of(name)],
             device_id=dev, device_id_type=MESH,
@@ -125,14 +125,24 @@
     def tg_of(k):
         return tg.at[c, (y + NY - k) % NY]
 
-    for k in (4, 3, 5, 2, 6, 1, 7):
+    @pl.when(c == 0)
+    def _():
+        send(tg_of(0), tg_of(0), ("tg", 4), yat(4), count=False)
+
+    for k in (3, 5, 2, 6, 1, 7):
         send(tg_of(0), tg_of(0), ("tg", k), yat(k))
     send(tg_of(0), tg_of(0), ("tgm",), mate)
-    for k in (1, 7, 2, 6, 3, 5, 4):
+    for k in (5, 3, 1, 7, 2, 6, 4):
         wait(tg_of(k), ("tg", k))
+        if k == 5:
+
+            @pl.when(c == 1)
+            def _():
+                send(tg_of(5), tg_of(5), ("tg", 4), yat(7))
+
         send(tg_of(k), tg_of(k), ("tgm",), mate)
     loads["sr"].wait()
-    for k in (3, 5, 2, 6, 1, 7):
+    for k in (2, 6, 1, 7):
         send(sg.at[0], sg.at[k], ("sg", k), yat(k))
     send(sg.at[0], sg.at[8], ("sgm",), mate)
     phase("tgmate")
@@ -143,12 +153,13 @@
         rows = tg[s % 2, s // 2].astype(F32)
         xn[4 * s : 4 * s + 4] = rows[0:4]
         xo[4 * s : 4 * s + 4] = rows[4:8]
-    loads["q"].wait()
-    queries = nn(xn[...].astype(BF16), wq[...]).astype(BF16)
-    zf[0, x, 0:64] = queries
     loads["o"].wait()
     hgrad = nt(xo[...].astype(BF16), wo[...]).astype(BF16)
     xf[0, x] = hgrad
+    for e in (2, 1, 3):
+        send(xf.at[0, x], xf.at[0, x], ("xfx", e), xat(e))
+    loads["q"].wait()
+    zf[0, x, 0:64] = nn(xn[...].astype(BF16), wq[...]).astype(BF16)
     loads["sv"].wait()
     loads["of"].wait()
     deltas = jnp.sum(hgrad.astype(F32) * sv[...].astype(F32), axis=1, keepdims=True)
@@ -163,7 +174,11 @@
     def xs(e):
         return (x + NX - e) % NX
 
+    straight = (3, 5, 4)
+
     def zf_x(k):
+        if k in straight:
+            send(zf.at[k, x], zf.at[k, x], ("zfx", k, 2), xat(2))
         send(zf.at[k, x], zf.at[k, x], ("zfx", k, 1), xat(1))
         send(zf.at[k, x], zf.at[k, x], ("zfx", k, 3), xat(3))
 
@@ -178,27 +193,33 @@
     def zf_relay(k):
         wait(zf.at[k, xs(1)], ("zfx", k, 1))
         wait(zf.at[k, xs(3)], ("zfx", k, 3))
-        e = 1 if k % 2 == 0 else 3
-        send(zf.at[k, xs(e)], zf.at[k, xs(e)], ("zfx", k, 2), xat(e))
+        if k not in straight:
+            e = 1 if k % 2 == 0 else 3
+            send(zf.at[k, xs(e)], zf.at[k, xs(e)], ("zfx", k, 2), xat(e))
 
     def zf_end(k):
+        if k in straight:
+            zf_relay(k)
         wait(zf.at[k, xs(2)], ("zfx", k, 2))
 
     def xf_z(k, e):
         if k:
             wait(xf.at[k, xs(e)], ("xfz", k, e))
-        if k <= 2:
+        if k <= 2 or (k == 3 and e % 2 == 0):
             send(xf.at[k, xs(e)], xf.at[k + 1, xs(e)], ("xfz", k + 1, e), zat(1))
-        if k == 0 or k >= 5:
+        if k == 0 or k >= 6 or (k == 5 and e % 2 == 1):
             send(xf.at[k, xs(e)], xf.at[(k - 1) % NZ, xs(e)], ("xfz", (k - 1) % NZ, e), zat(7))
 
     def sg_in(k):
         wait(sg.at[k], ("sg", k))
+        if k == 2:
+            send(sg.at[2], sg.at[3], ("sg", 3), yat(1))
+        if k == 6:
+            send(sg.at[6], sg.at[5], ("sg", 5), yat(7))
+            send(sg.at[2 + 4 * c], sg.at[4], ("sg", 4), (z, x, ((y + NY + 2 * way) % NY) * 2 + c))
         send(sg.at[k], sg.at[8 + k], ("sgm",), mate)
 
     phase("spsend")
-    send(xf.at[0, x], xf.at[0, x], ("xfx", 1), xat(1))
-    send(xf.at[0, x], xf.at[0, x], ("xfx", 3), xat(3))
     zf_z(0)
     xf_z(0, 0)
     zf_x(0)
@@ -206,79 +227,95 @@
     phase("step1")
     for f in range(8):
         nb[f] = xn[:, 256 * f : 256 * f + 256].astype(BF16)
-    wait(xf.at[0, xs(1)], ("xfx", 1))
-    xf_z(0, 1)
-    wait(xf.at[0, xs(3)], ("xfx", 3))
-    send(xf.at[0, xs(3)], xf.at[0, xs(3)], ("xfx", 2), xat(3))
-    xf_z(0, 3)
-    zf_z(1)
-    zf_z(7)
-    zf_x(1)
-    zf_x(7)
+    for e in (1, 3):
+        wait(xf.at[0, xs(e)], ("xfx", e))
+        xf_z(0, e)
+    for k in (1, 7):
+        zf_z(k)
+    wait(xf.at[0, xs(2)], ("xfx", 2))
+    xf_z(0, 2)
+    for k in (1, 7):
+        xf_z(k, 0)
+    for k in (1, 7):
+        zf_x(k)
     zf_relay(0)
+    sg_in(2)
+    sg_in(6)
+    phase("step2")
+    for e in (1, 3):
+        xf_z(1, e)
+        xf_z(7, e)
+    for k in (2, 6):
+        zf_z(k)
+        xf_z(k, 0)
+    for k in (1, 7):
+        xf_z(k, 2)
+    for k in (2, 6):
+        zf_x(k)
+    zf_relay(1)
+    zf_relay(7)
     sg_in(1)
     sg_in(7)
-    wait(xf.at[0, xs(2)], ("xfx", 2))
-    xf_z(0, 2)
-    phase("step2")
-    for e in (0, 1, 3, 2):
-        xf_z(1, e)
-        xf_z(7, e)
-    zf_z(2)
-    zf_z(6)
-    zf_x(2)
-    zf_x(6)
-    sg_in(2)
-    sg_in(6)
-    zf_relay(1)
-    zf_relay(7)
     phase("step3")
-    for e in (0, 1, 3, 2):
+    for e in (1, 3):
         xf_z(2, e)
         xf_z(6, e)
+    for k in (3, 5):
+        zf_z(k)
+        xf_z(k, 0)
+    for k in (2, 6):
+        xf_z(k, 2)
+    for k in (3, 5):
+        zf_x(k)
+    zf_relay(2)
+    zf_relay(6)
     sg_in(3)
     sg_in(5)
-    send(sg.at[3 + 2 * c], sg.at[4], ("sg", 4), (z, x, ((y + NY + way) % NY) * 2 + c))
-    zf_z(3)
-    zf_z(5)
-    zf_x(3)
-    zf_x(5)
-    zf_relay(2)
-    zf_relay(6)
     sg_in(4)
     phase("step4")
-    for e in (0, 1, 3, 2):
+    for e in (1, 3):
         xf_z(3, e)
         xf_z(5, e)
     zf_z(4)
     zf_x(4)
+    for k in (3, 5):
+        xf_z(k, 2)
     for k in range(1, NZ):
         send(nb.at[(z + k) % NZ], nr.at[k], ("nb",), zat(k))
     phase("kproj")
     wait(sg.at[8:16], ("sgm",))
     loads["k"].wait()
     kb[...] = nn(sg[...].reshape(256, 2048), wk[...]).astype(BF16)
-    zf_relay(3)
-    zf_relay(5)
     phase("vproj")
     loads["v"].wait()
     vb[...] = nn(sg[...].reshape(256, 2048), wv[...]).astype(BF16)
-    zf_relay(4)
+
+    back = {2: 3, 6: 3, 3: 3, 5: 3}
 
     def x_sends(k):
-        e = 1 if k % 2 == 0 else 3
-        send(part.at[k, (x + 2) % NX], reli.at[k], ("rel", k), xat(e))
-        send(part.at[k, (x + 4 - e) % NX], xin.at[k, 1], ("xin", k), xat(4 - e))
+        e = back.get(k)
+        if e is None:
+            for e in (2, 1, 3):
+                send(part.at[k, (x + e) % NX], xin.at[k, e - 1], ("xin", k), xat(e))
+        else:
+            send(part.at[k, (x + 2) % NX], reli.at[k], ("rel", k), xat(e))
+            send(part.at[k, (x + 4 - e) % NX], xin.at[k, 1], ("xin", k), xat(4 - e))
 
     def x_relay(k):
-        e = 1 if k % 2 == 0 else 3
+        e = back.get(k)
+        if e is None:
+            return
         wait(reli.at[k], ("rel", k))
         relo[k] = (part[k, (x + e) % NX].astype(F32) + reli[k].astype(F32)).astype(BF16)
         send(relo.at[k], xin.at[k, 0], ("xin", k), xat(e))
 
     def x_sum(k):
-        wait(xin.at[k], ("xin", k))
-        return part[k, x].astype(F32) + xin[k, 0].astype(F32) + xin[k, 1].astype(F32)
+        count = 2 if k in back else 3
+        wait(xin.at[k, 0:count], ("xin", k))
+        total = part[k, x].astype(F32)
+        for n in range(count):
+            total += xin[k, n].astype(F32)
+        return total
 
     def z_send(k):
         if k:
@@ -304,21 +341,31 @@
         dq = nn(jnp.transpose(grad).astype(BF16), kb[...])
         part[k] = dq.astype(BF16).reshape(4, 64, 256)
 
-    order = (1, 7, 2, 6, 0, 3, 5, 4)
-    for n, k in enumerate(order):
-        phase(f"group{n}")
-        if k == 3:
+    def work(k, first=False):
+        phase(f"group{k}")
+        if k == 4:
             for e in range(4):
                 xf_z(4, e)
         zf_end(k)
-        group(k, n == 0)
-        x_sends(k)
-        if n >= 3:
-            phase(f"relay{n - 3}")
-            x_relay(order[n - 3])
-        if n >= 6:
-            phase(f"zsend{n - 6}")
-            z_send(order[n - 6])
+        group(k, first)
+        if k in (1, 7):
+            send(part.at[k], near.at[k // 7], ("near", k), zat(NZ - k))
+        elif k:
+            x_sends(k)
+
+    for k in (2, 6, 1, 7, 3):
+        work(k, k == 2)
+    phase("relay2")
+    x_relay(2)
+    work(5)
+    phase("relay6")
+    x_relay(6)
+    work(4)
+    work(0)
+    phase("relay3")
+    x_relay(3)
+    phase("zsend2")
+    z_send(2)
 
     phase("gmat1")
     dkb = dk[...].astype(BF16)
@@ -337,40 +384,48 @@
     gmat(1)
     send(gout.at[1], gin, ("gm",), mate)
     phase("relay5")
-    x_relay(order[5])
-    z_send(order[2])
-    z_send(order[3])
-    phase("relay6")
-    x_relay(order[6])
+    x_relay(5)
+    phase("zsend6")
+    z_send(6)
+    phase("near")
+    wait(near.at[0], ("near", 1))
+    wait(near.at[1], ("near", 7))
+    part[0] = (part[0].astype(F32) + near[0].astype(F32) + near[1].astype(F32)).astype(BF16)
+    x_sends(0)
     phase("gmat0")
     gmat(0)
-    phase("relay7")
-    x_relay(order[7])
-    z_send(order[5])
+    phase("zsend3")
+    z_send(3)
+    phase("zsend5")
+    z_send(5)
+    phase("zsend4")
+    z_send(4)
+    phase("gsum")
+    wait(gin, ("gm",))
+    for k in (4, 3, 5, 2, 6, 1, 7):
+        gsum[k] = (gout[0, k].astype(F32) + gin[k].astype(F32)).astype(BF16)
+        send(gsum.at[k], grecv.at[k], ("g",), yat(NY - k))
+
     phase("nrt")
     nr[0] = nb[z]
     wait(nr.at[1:8], ("nb",))
     for j in range(4):
         pair = nr[2 * j : 2 * j + 2].reshape(128, 256).astype(F32)
         nrt[:, 128 * j : 128 * j + 128] = pair.T.astype(BF16)
-    phase("zsend")
-    z_send(order[6])
-    z_send(order[7])
-    phase("gsum")
-    wait(gin, ("gm",))
-    for k in (4, 3, 5, 2, 6, 1, 7):
-        gsum[k] = (gout[0, k].astype(F32) + gin[k].astype(F32)).astype(BF16)
-        send(gsum.at[k], grecv.at[k], ("g",), yat(NY - k))
-
     phase("qflat")
     total = x_sum(0)
-    wait(zin.at[1:8], ("zin",))
-    for k in range(1, NZ):
+    wait(zin.at[2:7], ("zin",))
+    for k in range(2, 7):
         total += zin[k].astype(F32)
     qflat = total.astype(BF16)
     qz[0] = qflat
-    for k in (4, 3, 5, 2, 6, 1, 7):
-        send(qz.at[0], qz.at[k], ("qz",), zat(k))
+
+    @pl.when(c == 0)
+    def _():
+        send(qz.at[0], qz.at[4], ("qz", 4), zat(4), count=False)
+
+    for k in (3, 5, 2, 6, 1, 7):
+        send(qz.at[0], qz.at[k], ("qz", k), zat(k))
 
     phase("ng")
     for f in range(2):
@@ -387,7 +442,14 @@
         send(nsum.at[(y + NY - k) % NY], nrecv.at[k], ("n",), yat(NY - k))
 
     phase("wmat")
-    wait(qz.at[1:8], ("qz",))
+    wait(qz.at[5], ("qz", 5))
+
+    @pl.when(c == 1)
+    def _():
+        send(qz.at[5], qz.at[4], ("qz", 4), zat(7))
+
+    for k in (1, 7, 2, 6, 3, 4):
+        wait(qz.at[k], ("qz", k))
     wsum = nn(nrt[...], qz[...].reshape(512, 256))
     wpart[...] = wsum.astype(BF16).reshape(4, 64, 256)
     for e in (2, 1, 3):
@@ -446,7 +508,7 @@
     )
     results = pl.pallas_call(
         kernel,
-        out_shape=outs,
+        out_shape=tuple(pltpu.VMEM(o.shape, o.dtype) for o in outs),
         in_specs=[hb] * 10,
         out_specs=(vm, vm, vm),
         scratch_shapes=[
@@ -457,7 +519,8 @@
             buf(8, 4, 80, 256), buf(8, 4, 64, 256),
             buf(256, 256), buf(256, 256),
             buf(256, 256, dtype=F32), buf(256, 256, dtype=F32),
-            buf(8, 4, 64, 256), buf(8, 64, 256), buf(8, 64, 256), buf(8, 2, 64, 256),
+            buf(8, 4, 64, 256), buf(2, 4, 64, 256), buf(8, 64, 256), buf(8, 64, 256),
+            buf(8, 3, 64, 256),
             buf(8, 64, 256), buf(8, 64, 256),
             buf(8, 64, 256), buf(4, 64, 256), buf(4, 64, 256),
             buf(2, 8, 16, 2048), buf(8, 16, 2048), buf(8, 16, 2048), buf(8, 16, 2048),
@@ -473,7 +536,7 @@
     )(tr, sr, gain.reshape(16, 128), wq, wk, wv, wo, saved, offset.reshape(1, 64), og)
     return pl.pallas_call(
         finish, out_shape=outs, in_specs=[vm, vm, vm], out_specs=(vm, vm, vm)
-    )(*results)
+    )(*[pltpu.with_memory_space_constraint(r, pltpu.VMEM) for r in results])
 
 
 def solution(mesh):

time: 81.9 us -> 75.3 us (0.919)
  the two profiles are of different devices: /device:TPU:2 before, /device:TPU:1 now
where the time goes in v3:
time: 75.3 us; the launch traced here: 75 us
  Pallas kernels  74.4 us (99%)
    pallas_call x1, Pallas kernels, body(): pl.pallas_call(kernel, out_shape=tuple((pltpu.VMEM(o.shape, o.dtype) for...  73.7 us

profile of v3, /device:TPU:1, one launch (start us, length us, event | category | flops | bytes accessed | tf_op | source)
XLA Modules:
  0.0 75.0 jit_solution(8367233817785111040)
XLA Ops:
  0.6 73.7 %shard_map.121 = (f32[4,2048]{1,0:T(4,128)S(1)}, f32[16,2048]{1,0:T(8,128)S(1)}, f32[64,256]{1,0:T(8,128)S(1)}) custom-call(bf16[4,2048]{1,0:T(4,128)(2,1)} %tr_hbm.1, bf16[16,2048]{1,0:T(8,128)(2,1)} %sr_hbm.1, bf16[16,128]{1,0:T(8,128)(2,1)} %bitcast.2, bf16[2048,256]{1,0:T(8,128)(2,1)} %wq_hbm.1, bf16[2048,256]{1,0:T(8,128)(2,1)} %wk_hbm.1, ...), custom_call_target="tpu_custom_call" | custom-call | tf_op jit(solution)/shard_map/pallas_call | solution.py:509
  74.3 0.7 shard_map.122

commit v4 on v3

--- a/solution.py
+++ b/solution.py
@@ -17,8 +17,8 @@
 F32 = jnp.float32
 BF16 = jnp.bfloat16
 NZ, NX, NY = 8, 4, 8
-UNIT = 8192
-UNITS = 1024
+UNIT = 2048
+UNITS = 4096
 RECVS = 112
 
 
@@ -34,10 +34,10 @@
     tr_hbm, sr_hbm, gain_hbm, wq_hbm, wk_hbm, wv_hbm, wo_hbm, saved_hbm, off_hbm, og_hbm,
     tgrad_ref, sgrad_ref, wgrad_ref,
     tr, gn, sv, of, og,
-    tg, xn, xo, nb, nr, nrt, sg, wq, wk, wv, wo, zf, xf, kb, vb, dk, dv,
-    part, near, reli, relo, xin, zout, zin,
+    tg, xn, xo, nzs, nza, nyb, nr, nrt, sg, wq, wk, wv, wo, zf, xf, kb, vb, dk, dv,
+    part, near, xin, zout, zin,
     qz, wpart, win,
-    gout, gin, gsum, grecv, nout, nin, nsum, nrecv,
+    gout, gin, gsum, gmid, grecv, nout, nin, nsum, nrecv,
     units, ssem, rsem, lsem,
 ):
     z = lax.axis_index("sp_0")
@@ -114,9 +114,10 @@
     gain = jnp.concatenate([gain[s : s + 1] for s in range(16)], axis=1)
     target = tr[...].astype(F32)
     inverse = lax.rsqrt(jnp.mean(target * target, axis=1, keepdims=True) + EPSILON)
-    tg[c, y] = jnp.concatenate(
-        [target * inverse * gain, og[...].astype(F32)], axis=0
-    ).astype(BF16)
+    normed = target * inverse * gain
+    tg[c, y] = jnp.concatenate([normed, og[...].astype(F32)], axis=0).astype(BF16)
+    for f in range(NZ):
+        nzs[f] = normed[:, 256 * f : 256 * f + 256].astype(BF16)
     phase("barrier")
     pl.semaphore_wait(barrier, len(peers))
 
@@ -125,21 +126,13 @@
     def tg_of(k):
         return tg.at[c, (y + NY - k) % NY]
 
-    @pl.when(c == 0)
-    def _():
-        send(tg_of(0), tg_of(0), ("tg", 4), yat(4), count=False)
-
-    for k in (3, 5, 2, 6, 1, 7):
+    for k in (4, 3, 5, 2, 6, 1, 7):
         send(tg_of(0), tg_of(0), ("tg", k), yat(k))
     send(tg_of(0), tg_of(0), ("tgm",), mate)
-    for k in (5, 3, 1, 7, 2, 6, 4):
+    for k in range(1, NZ):
+        send(nzs.at[(z + k) % NZ], nza.at[k], ("nza",), zat(k))
+    for k in (1, 7, 2, 6, 3, 5, 4):
         wait(tg_of(k), ("tg", k))
-        if k == 5:
-
-            @pl.when(c == 1)
-            def _():
-                send(tg_of(5), tg_of(5), ("tg", 4), yat(7))
-
         send(tg_of(k), tg_of(k), ("tgm",), mate)
     loads["sr"].wait()
     for k in (2, 6, 1, 7):
@@ -174,13 +167,9 @@
     def xs(e):
         return (x + NX - e) % NX
 
-    straight = (3, 5, 4)
-
     def zf_x(k):
-        if k in straight:
-            send(zf.at[k, x], zf.at[k, x], ("zfx", k, 2), xat(2))
-        send(zf.at[k, x], zf.at[k, x], ("zfx", k, 1), xat(1))
-        send(zf.at[k, x], zf.at[k, x], ("zfx", k, 3), xat(3))
+        for e in (2, 1, 3):
+            send(zf.at[k, x], zf.at[k, x], ("zfx", k, e), xat(e))
 
     def zf_z(k):
         if k:
@@ -190,17 +179,9 @@
         if k == 0 or k >= 6:
             send(zf.at[k, x], zf.at[(k - 1) % NZ, x], ("zfz", (k - 1) % NZ), zat(7))
 
-    def zf_relay(k):
-        wait(zf.at[k, xs(1)], ("zfx", k, 1))
-        wait(zf.at[k, xs(3)], ("zfx", k, 3))
-        if k not in straight:
-            e = 1 if k % 2 == 0 else 3
-            send(zf.at[k, xs(e)], zf.at[k, xs(e)], ("zfx", k, 2), xat(e))
-
     def zf_end(k):
-        if k in straight:
-            zf_relay(k)
-        wait(zf.at[k, xs(2)], ("zfx", k, 2))
+        for e in (1, 3, 2):
+            wait(zf.at[k, xs(e)], ("zfx", k, e))
 
     def xf_z(k, e):
         if k:
@@ -219,101 +200,14 @@
             send(sg.at[2 + 4 * c], sg.at[4], ("sg", 4), (z, x, ((y + NY + 2 * way) % NY) * 2 + c))
         send(sg.at[k], sg.at[8 + k], ("sgm",), mate)
 
-    phase("spsend")
-    zf_z(0)
-    xf_z(0, 0)
-    zf_x(0)
-
-    phase("step1")
-    for f in range(8):
-        nb[f] = xn[:, 256 * f : 256 * f + 256].astype(BF16)
-    for e in (1, 3):
-        wait(xf.at[0, xs(e)], ("xfx", e))
-        xf_z(0, e)
-    for k in (1, 7):
-        zf_z(k)
-    wait(xf.at[0, xs(2)], ("xfx", 2))
-    xf_z(0, 2)
-    for k in (1, 7):
-        xf_z(k, 0)
-    for k in (1, 7):
-        zf_x(k)
-    zf_relay(0)
-    sg_in(2)
-    sg_in(6)
-    phase("step2")
-    for e in (1, 3):
-        xf_z(1, e)
-        xf_z(7, e)
-    for k in (2, 6):
-        zf_z(k)
-        xf_z(k, 0)
-    for k in (1, 7):
-        xf_z(k, 2)
-    for k in (2, 6):
-        zf_x(k)
-    zf_relay(1)
-    zf_relay(7)
-    sg_in(1)
-    sg_in(7)
-    phase("step3")
-    for e in (1, 3):
-        xf_z(2, e)
-        xf_z(6, e)
-    for k in (3, 5):
-        zf_z(k)
-        xf_z(k, 0)
-    for k in (2, 6):
-        xf_z(k, 2)
-    for k in (3, 5):
-        zf_x(k)
-    zf_relay(2)
-    zf_relay(6)
-    sg_in(3)
-    sg_in(5)
-    sg_in(4)
-    phase("step4")
-    for e in (1, 3):
-        xf_z(3, e)
-        xf_z(5, e)
-    zf_z(4)
-    zf_x(4)
-    for k in (3, 5):
-        xf_z(k, 2)
-    for k in range(1, NZ):
-        send(nb.at[(z + k) % NZ], nr.at[k], ("nb",), zat(k))
-    phase("kproj")
-    wait(sg.at[8:16], ("sgm",))
-    loads["k"].wait()
-    kb[...] = nn(sg[...].reshape(256, 2048), wk[...]).astype(BF16)
-    phase("vproj")
-    loads["v"].wait()
-    vb[...] = nn(sg[...].reshape(256, 2048), wv[...]).astype(BF16)
-
-    back = {2: 3, 6: 3, 3: 3, 5: 3}
-
     def x_sends(k):
-        e = back.get(k)
-        if e is None:
-            for e in (2, 1, 3):
-                send(part.at[k, (x + e) % NX], xin.at[k, e - 1], ("xin", k), xat(e))
-        else:
-            send(part.at[k, (x + 2) % NX], reli.at[k], ("rel", k), xat(e))
-            send(part.at[k, (x + 4 - e) % NX], xin.at[k, 1], ("xin", k), xat(4 - e))
-
-    def x_relay(k):
-        e = back.get(k)
-        if e is None:
-            return
-        wait(reli.at[k], ("rel", k))
-        relo[k] = (part[k, (x + e) % NX].astype(F32) + reli[k].astype(F32)).astype(BF16)
-        send(relo.at[k], xin.at[k, 0], ("xin", k), xat(e))
+        for e in (2, 1, 3):
+            send(part.at[k, (x + e) % NX], xin.at[k, e - 1], ("xin", k), xat(e))
 
     def x_sum(k):
-        count = 2 if k in back else 3
-        wait(xin.at[k, 0:count], ("xin", k))
+        wait(xin.at[k], ("xin", k))
         total = part[k, x].astype(F32)
-        for n in range(count):
+        for n in range(3):
             total += xin[k, n].astype(F32)
         return total
 
@@ -343,29 +237,92 @@
 
     def work(k, first=False):
         phase(f"group{k}")
-        if k == 4:
-            for e in range(4):
-                xf_z(4, e)
         zf_end(k)
         group(k, first)
-        if k in (1, 7):
-            send(part.at[k], near.at[k // 7], ("near", k), zat(NZ - k))
-        elif k:
+        if k not in (0, 1, 7):
             x_sends(k)
 
-    for k in (2, 6, 1, 7, 3):
-        work(k, k == 2)
-    phase("relay2")
-    x_relay(2)
+    phase("spsend")
+    zf_z(0)
+    xf_z(0, 0)
+    zf_x(0)
+
+    phase("step1")
+    for e in (1, 3):
+        wait(xf.at[0, xs(e)], ("xfx", e))
+        xf_z(0, e)
+    for k in (1, 7):
+        zf_z(k)
+    wait(xf.at[0, xs(2)], ("xfx", 2))
+    xf_z(0, 2)
+    for k in (1, 7):
+        xf_z(k, 0)
+    for k in (1, 7):
+        zf_x(k)
+    sg_in(2)
+    sg_in(6)
+    phase("step2")
+    for e in (1, 3):
+        xf_z(1, e)
+        xf_z(7, e)
+    for k in (2, 6):
+        zf_z(k)
+        xf_z(k, 0)
+    for k in (1, 7):
+        xf_z(k, 2)
+    for k in (2, 6):
+        zf_x(k)
+    for k in (1, 7, 3, 5, 4):
+        sg_in(k)
+    nza[0] = nzs[z]
+    wait(nza.at[1:8], ("nza",))
+    nyb[c, y] = nza[...]
+    for k in (4, 3, 5, 2, 6, 1, 7):
+        send(nza, nyb.at[c, y], ("nyb",), yat(k))
+    send(nza, nyb.at[c, y], ("nybm",), mate)
+    phase("step3")
+    for e in (1, 3):
+        xf_z(2, e)
+        xf_z(6, e)
+    for k in (3, 5):
+        zf_z(k)
+        xf_z(k, 0)
+    for k in (2, 6):
+        xf_z(k, 2)
+    for k in (3, 5):
+        zf_x(k)
+    phase("kproj")
+    wait(sg.at[8:16], ("sgm",))
+    loads["k"].wait()
+    kb[...] = nn(sg[...].reshape(256, 2048), wk[...]).astype(BF16)
+    phase("vproj")
+    loads["v"].wait()
+    vb[...] = nn(sg[...].reshape(256, 2048), wv[...]).astype(BF16)
+    work(1, True)
+    work(7)
+    phase("step4")
+    for e in (1, 3):
+        xf_z(3, e)
+        xf_z(5, e)
+    zf_z(4)
+    zf_x(4)
+    for k in (3, 5):
+        xf_z(k, 2)
+    for k in (1, 7):
+        send(part.at[k], near.at[k // 7], ("near", k), zat(NZ - k))
+    phase("nyb")
+    wait(nyb.at[0, 0:7], ("nyb",))
+    for k in range(1, NY):
+        send(nyb.at[c, (y + k) % NY], nyb.at[c, (y + k) % NY], ("nybm",), mate)
+    work(2)
+    work(6)
+    work(0)
+    phase("xf4")
+    for e in range(4):
+        xf_z(4, e)
+    work(3)
     work(5)
-    phase("relay6")
-    x_relay(6)
     work(4)
-    work(0)
-    phase("relay3")
-    x_relay(3)
-    phase("zsend2")
-    z_send(2)
 
     phase("gmat1")
     dkb = dk[...].astype(BF16)
@@ -383,8 +340,10 @@
 
     gmat(1)
     send(gout.at[1], gin, ("gm",), mate)
-    phase("relay5")
-    x_relay(5)
+    phase("zsend2")
+    z_send(2)
+    phase("gmat0")
+    gmat(0)
     phase("zsend6")
     z_send(6)
     phase("near")
@@ -392,26 +351,30 @@
     wait(near.at[1], ("near", 7))
     part[0] = (part[0].astype(F32) + near[0].astype(F32) + near[1].astype(F32)).astype(BF16)
     x_sends(0)
-    phase("gmat0")
-    gmat(0)
     phase("zsend3")
     z_send(3)
     phase("zsend5")
     z_send(5)
     phase("zsend4")
     z_send(4)
+    phase("nrt")
+    wait(nyb.at[0], ("nybm",))
+    for s in range(16):
+        rows = nyb[s % 2, s // 2].astype(F32)
+        for k in range(NZ):
+            nr[k, 4 * s : 4 * s + 4] = rows[k]
+    for j in range(4):
+        pair = nr[2 * j : 2 * j + 2].reshape(128, 256)
+        nrt[:, 128 * j : 128 * j + 128] = pair.T.astype(BF16)
     phase("gsum")
     wait(gin, ("gm",))
-    for k in (4, 3, 5, 2, 6, 1, 7):
+    for k in (4, 3, 5, 1, 7):
         gsum[k] = (gout[0, k].astype(F32) + gin[k].astype(F32)).astype(BF16)
-        send(gsum.at[k], grecv.at[k], ("g",), yat(NY - k))
-
-    phase("nrt")
-    nr[0] = nb[z]
-    wait(nr.at[1:8], ("nb",))
-    for j in range(4):
-        pair = nr[2 * j : 2 * j + 2].reshape(128, 256).astype(F32)
-        nrt[:, 128 * j : 128 * j + 128] = pair.T.astype(BF16)
+    send(gsum.at[4], gmid.at[2], ("gmid",), yat((NY - 2 * way) % NY))
+    send(gsum.at[3], gmid.at[0], ("gmid",), yat(7))
+    send(gsum.at[5], gmid.at[1], ("gmid",), yat(1))
+    send(gsum.at[1], grecv.at[1], ("g",), yat(7))
+    send(gsum.at[7], grecv.at[7], ("g",), yat(1))
     phase("qflat")
     total = x_sum(0)
     wait(zin.at[2:7], ("zin",))
@@ -420,12 +383,8 @@
     qflat = total.astype(BF16)
     qz[0] = qflat
 
-    @pl.when(c == 0)
-    def _():
-        send(qz.at[0], qz.at[4], ("qz", 4), zat(4), count=False)
-
-    for k in (3, 5, 2, 6, 1, 7):
-        send(qz.at[0], qz.at[k], ("qz", k), zat(k))
+    for k in (4, 3, 5, 2, 6, 1, 7):
+        send(qz.at[0], qz.at[k], ("qz",), zat(k))
 
     phase("ng")
     for f in range(2):
@@ -435,6 +394,12 @@
                 [half[4 * s : 4 * s + 4] for half in halves], axis=0
             ).astype(BF16)
     send(nout.at[1 - c], nin, ("nm",), mate)
+    phase("gmid")
+    wait(gmid, ("gmid",))
+    for k, n in ((2, 0), (6, 1)):
+        mid = jnp.where(c == n, gmid[2].astype(F32), 0.0) + gmid[n].astype(F32)
+        gsum[k] = (gout[0, k].astype(F32) + gin[k].astype(F32) + mid).astype(BF16)
+        send(gsum.at[k], grecv.at[k], ("g",), yat(NY - k))
     phase("nsum")
     wait(nin, ("nm",))
     nsum[...] = (nout[c].astype(F32) + nin[...].astype(F32)).astype(BF16)
@@ -442,23 +407,16 @@
         send(nsum.at[(y + NY - k) % NY], nrecv.at[k], ("n",), yat(NY - k))
 
     phase("wmat")
-    wait(qz.at[5], ("qz", 5))
-
-    @pl.when(c == 1)
-    def _():
-        send(qz.at[5], qz.at[4], ("qz", 4), zat(7))
-
-    for k in (1, 7, 2, 6, 3, 4):
-        wait(qz.at[k], ("qz", k))
+    wait(qz.at[1:8], ("qz",))
     wsum = nn(nrt[...], qz[...].reshape(512, 256))
     wpart[...] = wsum.astype(BF16).reshape(4, 64, 256)
     for e in (2, 1, 3):
         send(wpart.at[(x + e) % NX], win.at[e], ("w",), xat(e))
 
     phase("gfin")
-    wait(grecv.at[1:8], ("g",))
+    wait(grecv.at[0:4], ("g",))
     total = gout[0, 0].astype(F32) + gin[0].astype(F32)
-    for k in range(1, NY):
+    for k in (1, 2, 6, 7):
         total += grecv[k].astype(F32)
     sgrad_ref[...] = total
 
@@ -514,18 +472,19 @@
         scratch_shapes=[
             buf(4, 2048), buf(16, 128), buf(64, 256), buf(1, 64), buf(4, 2048),
             buf(2, 8, 8, 2048), buf(64, 2048, dtype=F32), buf(64, 2048, dtype=F32),
-            buf(8, 64, 256), buf(8, 64, 256), buf(256, 512), buf(16, 16, 2048),
+            buf(8, 4, 256), buf(8, 4, 256), buf(2, 8, 8, 4, 256),
+            buf(8, 64, 256, dtype=F32), buf(256, 512), buf(16, 16, 2048),
             buf(2048, 256), buf(2048, 256), buf(2048, 256), buf(256, 2048),
             buf(8, 4, 80, 256), buf(8, 4, 64, 256),
             buf(256, 256), buf(256, 256),
             buf(256, 256, dtype=F32), buf(256, 256, dtype=F32),
-            buf(8, 4, 64, 256), buf(2, 4, 64, 256), buf(8, 64, 256), buf(8, 64, 256),
+            buf(8, 4, 64, 256), buf(2, 4, 64, 256),
             buf(8, 3, 64, 256),
             buf(8, 64, 256), buf(8, 64, 256),
             buf(8, 64, 256), buf(4, 64, 256), buf(4, 64, 256),
-            buf(2, 8, 16, 2048), buf(8, 16, 2048), buf(8, 16, 2048), buf(8, 16, 2048),
+            buf(2, 8, 16, 2048), buf(8, 16, 2048), buf(8, 16, 2048), buf(3, 16, 2048), buf(8, 16, 2048),
             buf(2, 8, 8, 1024), buf(8, 8, 1024), buf(8, 8, 1024), buf(8, 8, 1024),
-            buf(UNITS, 16, 256),
+            buf(UNITS, 4, 256),
             pltpu.SemaphoreType.DMA((1,)),
             pltpu.SemaphoreType.DMA((RECVS,)),
             pltpu.SemaphoreType.DMA((10,)),

time: 75.3 us -> 71.1 us (0.944)
  Pallas kernels: 74.4 us -> 70.3 us
    pallas_call x1, Pallas kernels: 73.7 us -> 69.6 us  [body(): pl.pallas_call(kernel, out_shape=tuple((pltpu.VMEM(o.shape, o.dtype) for...]
where the time goes in v4:
time: 71.1 us; the launch traced here: 70.9 us
  Pallas kernels  70.3 us (99%)
    pallas_call x1, Pallas kernels, body(): pl.pallas_call(kernel, out_shape=tuple((pltpu.VMEM(o.shape, o.dtype) for...  69.6 us

profile of v4, /device:TPU:1, one launch (start us, length us, event | category | flops | bytes accessed | tf_op | source)
XLA Modules:
  0.0 70.9 jit_solution(14572271275241382136)
XLA Ops:
  0.6 69.6 %shard_map.121 = (f32[4,2048]{1,0:T(4,128)S(1)}, f32[16,2048]{1,0:T(8,128)S(1)}, f32[64,256]{1,0:T(8,128)S(1)}) custom-call(bf16[4,2048]{1,0:T(4,128)(2,1)} %tr_hbm.1, bf16[16,2048]{1,0:T(8,128)(2,1)} %sr_hbm.1, bf16[16,128]{1,0:T(8,128)(2,1)} %bitcast.2, bf16[2048,256]{1,0:T(8,128)(2,1)} %wq_hbm.1, bf16[2048,256]{1,0:T(8,128)(2,1)} %wk_hbm.1, ...), custom_call_target="tpu_custom_call" | custom-call | tf_op jit(solution)/shard_map/pallas_call | solution.py:467
  70.2 0.7 shard_map.122

commit v5 on v4

--- a/solution.py
+++ b/solution.py
@@ -58,7 +58,7 @@
 
     mate = (z, x, t + way)
     names = {}
-    sent = [0]
+    sent = [0, 0]
     scope = [None]
 
     def phase(name):
@@ -76,11 +76,11 @@
             names[name] = len(names)
         return names[name]
 
-    def send(src, dst, name, dev, count=True):
+    def send(src, dst, name, dev, sem=0):
         assert size(src) % UNIT == 0
-        sent[0] += count * size(src) // UNIT
+        sent[sem] += size(src) // UNIT
         pltpu.make_async_remote_copy(
-            src_ref=src, dst_ref=dst, send_sem=ssem.at[0], recv_sem=rsem.at[slot_of(name)],
+            src_ref=src, dst_ref=dst, send_sem=ssem.at[sem], recv_sem=rsem.at[slot_of(name)],
             device_id=dev, device_id_type=MESH,
         ).start()
 
@@ -94,7 +94,7 @@
     loads = {}
     for k, (name, src, dst) in enumerate(
         (
-            ("tr", tr_hbm, tr), ("og", og_hbm, og), ("gn", gain_hbm, gn), ("sr", sr_hbm, sg.at[0]),
+            ("tr", tr_hbm, tr), ("og", og_hbm, og), ("gn", gain_hbm, gn), ("sr", sr_hbm, sg.at[c, 0]),
             ("of", off_hbm, of), ("sv", saved_hbm, sv),
             ("q", wq_hbm, wq), ("o", wo_hbm, wo), ("k", wk_hbm, wk), ("v", wv_hbm, wv),
         )
@@ -122,6 +122,8 @@
     pl.semaphore_wait(barrier, len(peers))
 
     phase("tgwait")
+    loads["sr"].wait()
+    send(sg.at[c, 0], sg.at[c, 0], ("sg0",), mate)
 
     def tg_of(k):
         return tg.at[c, (y + NY - k) % NY]
@@ -134,10 +136,13 @@
     for k in (1, 7, 2, 6, 3, 5, 4):
         wait(tg_of(k), ("tg", k))
         send(tg_of(k), tg_of(k), ("tgm",), mate)
-    loads["sr"].wait()
-    for k in (2, 6, 1, 7):
-        send(sg.at[0], sg.at[k], ("sg", k), yat(k))
-    send(sg.at[0], sg.at[8], ("sgm",), mate)
+
+    @pl.when(c == 1)
+    def _():
+        wait(sg.at[0, 0], ("sg0",))
+        for k in (2, 6, 1, 7):
+            send(sg.at[:, 0], sg.at[:, k], ("sg", k), yat(k), 1)
+
     phase("tgmate")
     wait(tg.at[1 - c], ("tgm",))
 
@@ -162,7 +167,7 @@
     place = lax.broadcasted_iota(jnp.int32, (64, 256), 1) == x * 64 + lax.broadcasted_iota(
         jnp.int32, (64, 256), 0
     )
-    zf[0, x, 64:80] = nn(both, place.astype(F32).astype(BF16)).astype(BF16)
+    zf[0, x, 64:72] = nn(both, place.astype(F32).astype(BF16))[0:8].astype(BF16)
 
     def xs(e):
         return (x + NX - e) % NX
@@ -191,14 +196,18 @@
         if k == 0 or k >= 6 or (k == 5 and e % 2 == 1):
             send(xf.at[k, xs(e)], xf.at[(k - 1) % NZ, xs(e)], ("xfz", (k - 1) % NZ, e), zat(7))
 
-    def sg_in(k):
-        wait(sg.at[k], ("sg", k))
-        if k == 2:
-            send(sg.at[2], sg.at[3], ("sg", 3), yat(1))
-        if k == 6:
-            send(sg.at[6], sg.at[5], ("sg", 5), yat(7))
-            send(sg.at[2 + 4 * c], sg.at[4], ("sg", 4), (z, x, ((y + NY + 2 * way) % NY) * 2 + c))
-        send(sg.at[k], sg.at[8 + k], ("sgm",), mate)
+    def sg_in(*ks):
+        @pl.when(c == 1)
+        def _():
+            for k in ks:
+                wait(sg.at[:, k], ("sg", k))
+                if k == 2:
+                    send(sg.at[:, 2], sg.at[:, 3], ("sg", 3), yat(1), 1)
+                    send(sg.at[0, 2], sg.at[0, 4], ("sg", 4), yat(2), 1)
+                if k == 6:
+                    send(sg.at[:, 6], sg.at[:, 5], ("sg", 5), yat(7), 1)
+                    send(sg.at[1, 6], sg.at[1, 4], ("sg", 4), yat(6), 1)
+                send(sg.at[:, k], sg.at[:, k], ("sgm",), mate, 1)
 
     def x_sends(k):
         for e in (2, 1, 3):
@@ -219,7 +228,7 @@
     def group(k, first):
         q = zf[k, :, 0:64, :].reshape(256, 256)
         h = xf[k].reshape(256, 256)
-        stat = jnp.sum(zf[k, :, 64:80, :].astype(F32), axis=0)
+        stat = jnp.sum(zf[k, :, 64:72, :].astype(F32), axis=0)
         score = nt(kb[...], q)
         prob = jnp.exp(score * SCALE - (SHIFT + stat[0:1]))
         grad = prob * (nt(vb[...], h) - stat[1:2]) * SCALE
@@ -253,14 +262,13 @@
         xf_z(0, e)
     for k in (1, 7):
         zf_z(k)
+    sg_in(2, 6)
     wait(xf.at[0, xs(2)], ("xfx", 2))
     xf_z(0, 2)
     for k in (1, 7):
         xf_z(k, 0)
     for k in (1, 7):
         zf_x(k)
-    sg_in(2)
-    sg_in(6)
     phase("step2")
     for e in (1, 3):
         xf_z(1, e)
@@ -272,14 +280,25 @@
         xf_z(k, 2)
     for k in (2, 6):
         zf_x(k)
-    for k in (1, 7, 3, 5, 4):
-        sg_in(k)
+    sg_in(1, 7, 3, 5, 4)
     nza[0] = nzs[z]
     wait(nza.at[1:8], ("nza",))
     nyb[c, y] = nza[...]
     for k in (4, 3, 5, 2, 6, 1, 7):
         send(nza, nyb.at[c, y], ("nyb",), yat(k))
     send(nza, nyb.at[c, y], ("nybm",), mate)
+    phase("kproj")
+
+    @pl.when(c == 0)
+    def _():
+        wait(sg.at[1, 0], ("sg0",))
+        wait(sg.at[:, 1:8], ("sgm",))
+
+    loads["k"].wait()
+    kb[...] = nn(sg[...].reshape(256, 2048), wk[...]).astype(BF16)
+    phase("vproj")
+    loads["v"].wait()
+    vb[...] = nn(sg[...].reshape(256, 2048), wv[...]).astype(BF16)
     phase("step3")
     for e in (1, 3):
         xf_z(2, e)
@@ -291,13 +310,6 @@
         xf_z(k, 2)
     for k in (3, 5):
         zf_x(k)
-    phase("kproj")
-    wait(sg.at[8:16], ("sgm",))
-    loads["k"].wait()
-    kb[...] = nn(sg[...].reshape(256, 2048), wk[...]).astype(BF16)
-    phase("vproj")
-    loads["v"].wait()
-    vb[...] = nn(sg[...].reshape(256, 2048), wv[...]).astype(BF16)
     work(1, True)
     work(7)
     phase("step4")
@@ -338,12 +350,12 @@
                 .reshape(8, 16, 512)
             )
 
-    gmat(1)
-    send(gout.at[1], gin, ("gm",), mate)
+    gmat(0)
     phase("zsend2")
     z_send(2)
     phase("gmat0")
-    gmat(0)
+    gmat(1)
+    send(gout.at[1 - c], gin, ("gm",), mate)
     phase("zsend6")
     z_send(6)
     phase("near")
@@ -369,7 +381,7 @@
     phase("gsum")
     wait(gin, ("gm",))
     for k in (4, 3, 5, 1, 7):
-        gsum[k] = (gout[0, k].astype(F32) + gin[k].astype(F32)).astype(BF16)
+        gsum[k] = (gout[c, k].astype(F32) + gin[k].astype(F32)).astype(BF16)
     send(gsum.at[4], gmid.at[2], ("gmid",), yat((NY - 2 * way) % NY))
     send(gsum.at[3], gmid.at[0], ("gmid",), yat(7))
     send(gsum.at[5], gmid.at[1], ("gmid",), yat(1))
@@ -398,7 +410,7 @@
     wait(gmid, ("gmid",))
     for k, n in ((2, 0), (6, 1)):
         mid = jnp.where(c == n, gmid[2].astype(F32), 0.0) + gmid[n].astype(F32)
-        gsum[k] = (gout[0, k].astype(F32) + gin[k].astype(F32) + mid).astype(BF16)
+        gsum[k] = (gout[c, k].astype(F32) + gin[k].astype(F32) + mid).astype(BF16)
         send(gsum.at[k], grecv.at[k], ("g",), yat(NY - k))
     phase("nsum")
     wait(nin, ("nm",))
@@ -415,7 +427,7 @@
 
     phase("gfin")
     wait(grecv.at[0:4], ("g",))
-    total = gout[0, 0].astype(F32) + gin[0].astype(F32)
+    total = gout[c, 0].astype(F32) + gin[0].astype(F32)
     for k in (1, 2, 6, 7):
         total += grecv[k].astype(F32)
     sgrad_ref[...] = total
@@ -437,13 +449,21 @@
     wgrad_ref[...] = total
 
     phase("sendwait")
-    all_sent = units.at[0 : sent[0]]
-    pltpu.make_async_remote_copy(
-        src_ref=all_sent, dst_ref=all_sent, send_sem=ssem.at[0], recv_sem=rsem.at[0],
-        device_id=mate, device_id_type=MESH,
-    ).wait_send()
+    def sent_all(sem):
+        whole = units.at[0 : sent[sem]]
+        pltpu.make_async_remote_copy(
+            src_ref=whole, dst_ref=whole, send_sem=ssem.at[sem], recv_sem=rsem.at[0],
+            device_id=mate, device_id_type=MESH,
+        ).wait_send()
+
+    sent_all(0)
+
+    @pl.when(c == 1)
+    def _():
+        sent_all(1)
+
     phase(None)
-    assert sent[0] <= UNITS and len(names) <= RECVS, (sent[0], len(names))
+    assert max(sent) <= UNITS and len(names) <= RECVS, (sent[0], len(names))
 
 
 def finish(a_ref, b_ref, c_ref, oa_ref, ob_ref, oc_ref):
@@ -473,9 +493,9 @@
             buf(4, 2048), buf(16, 128), buf(64, 256), buf(1, 64), buf(4, 2048),
             buf(2, 8, 8, 2048), buf(64, 2048, dtype=F32), buf(64, 2048, dtype=F32),
             buf(8, 4, 256), buf(8, 4, 256), buf(2, 8, 8, 4, 256),
-            buf(8, 64, 256, dtype=F32), buf(256, 512), buf(16, 16, 2048),
+            buf(8, 64, 256, dtype=F32), buf(256, 512), buf(2, 8, 16, 2048),
             buf(2048, 256), buf(2048, 256), buf(2048, 256), buf(256, 2048),
-            buf(8, 4, 80, 256), buf(8, 4, 64, 256),
+            buf(8, 4, 72, 256), buf(8, 4, 64, 256),
             buf(256, 256), buf(256, 256),
             buf(256, 256, dtype=F32), buf(256, 256, dtype=F32),
             buf(8, 4, 64, 256), buf(2, 4, 64, 256),
@@ -485,7 +505,7 @@
             buf(2, 8, 16, 2048), buf(8, 16, 2048), buf(8, 16, 2048), buf(3, 16, 2048), buf(8, 16, 2048),
             buf(2, 8, 8, 1024), buf(8, 8, 1024), buf(8, 8, 1024), buf(8, 8, 1024),
             buf(UNITS, 4, 256),
-            pltpu.SemaphoreType.DMA((1,)),
+            pltpu.SemaphoreType.DMA((2,)),
             pltpu.SemaphoreType.DMA((RECVS,)),
             pltpu.SemaphoreType.DMA((10,)),
         ],

time: 71.1 us -> 70.4 us (level)
  the two profiles are of different devices: /device:TPU:1 before, /device:TPU:8 now
where the time goes in v5:
time: 70.4 us; the launch traced here: 70.2 us
  Pallas kernels  69.5 us (99%)
    pallas_call x1, Pallas kernels, body(): pl.pallas_call(kernel, out_shape=tuple((pltpu.VMEM(o.shape, o.dtype) for...  68.9 us

profile of v5, /device:TPU:8, one launch (start us, length us, event | category | flops | bytes accessed | tf_op | source)
XLA Modules:
  0.0 70.2 jit_solution(17764799345370947514)
XLA Ops:
  0.6 68.9 %shard_map.121 = (f32[4,2048]{1,0:T(4,128)S(1)}, f32[16,2048]{1,0:T(8,128)S(1)}, f32[64,256]{1,0:T(8,128)S(1)}) custom-call(bf16[4,2048]{1,0:T(4,128)(2,1)} %tr_hbm.1, bf16[16,2048]{1,0:T(8,128)(2,1)} %sr_hbm.1, bf16[16,128]{1,0:T(8,128)(2,1)} %bitcast.2, bf16[2048,256]{1,0:T(8,128)(2,1)} %wq_hbm.1, bf16[2048,256]{1,0:T(8,128)(2,1)} %wk_hbm.1, ...), custom_call_target="tpu_custom_call" | custom-call | tf_op jit(solution)/shard_map/pallas_call | solution.py:487
  69.5 0.7 shard_map.122

commit v6 on v5

--- a/solution.py
+++ b/solution.py
@@ -34,9 +34,9 @@
     tr_hbm, sr_hbm, gain_hbm, wq_hbm, wk_hbm, wv_hbm, wo_hbm, saved_hbm, off_hbm, og_hbm,
     tgrad_ref, sgrad_ref, wgrad_ref,
     tr, gn, sv, of, og,
-    tg, xn, xo, nzs, nza, nyb, nr, nrt, sg, wq, wk, wv, wo, zf, xf, kb, vb, dk, dv,
+    tg, xn, xo, nzs, nza, nyb, nr, nrt, nxs, nxa, nyx, nrx, nrtx, sg, wq, wk, wv, wo, zf, xf, kb, vb, dk, dv,
     part, near, xin, zout, zin,
-    qz, wpart, win,
+    qz, qx, wz, wzin, wpart, win,
     gout, gin, gsum, gmid, grecv, nout, nin, nsum, nrecv,
     units, ssem, rsem, lsem,
 ):
@@ -91,6 +91,12 @@
         ).wait_recv()
 
     phase("start")
+    barrier = pltpu.get_barrier_semaphore()
+    peers = [mate] + [yat(k) for k in range(1, NY)] + [xat(k) for k in range(1, NX)]
+    peers += [zat(k) for k in range(1, NZ)]
+    for dev in peers:
+        pl.semaphore_signal(barrier, inc=1, device_id=dev, device_id_type=MESH)
+
     loads = {}
     for k, (name, src, dst) in enumerate(
         (
@@ -102,12 +108,6 @@
         loads[name] = pltpu.make_async_copy(src, dst, lsem.at[k])
         loads[name].start()
 
-    barrier = pltpu.get_barrier_semaphore()
-    peers = [mate] + [yat(k) for k in range(1, NY)] + [xat(k) for k in range(1, NX)]
-    peers += [zat(k) for k in range(1, NZ)]
-    for dev in peers:
-        pl.semaphore_signal(barrier, inc=1, device_id=dev, device_id_type=MESH)
-
     for name in ("tr", "og", "gn"):
         loads[name].wait()
     gain = gn[...].astype(F32)
@@ -118,6 +118,10 @@
     tg[c, y] = jnp.concatenate([normed, og[...].astype(F32)], axis=0).astype(BF16)
     for f in range(NZ):
         nzs[f] = normed[:, 256 * f : 256 * f + 256].astype(BF16)
+    for f in range(NX):
+        nxs[f] = jnp.concatenate(
+            [normed[:, 256 * g + 64 * f : 256 * g + 64 * f + 64] for g in range(NZ)], axis=1
+        ).astype(BF16)
     phase("barrier")
     pl.semaphore_wait(barrier, len(peers))
 
@@ -133,7 +137,9 @@
     send(tg_of(0), tg_of(0), ("tgm",), mate)
     for k in range(1, NZ):
         send(nzs.at[(z + k) % NZ], nza.at[k], ("nza",), zat(k))
-    for k in (1, 7, 2, 6, 3, 5, 4):
+    for e in range(1, NX):
+        send(nxs.at[(x + e) % NX], nxa.at[x], ("nxa",), xat(e))
+    for k in (3, 5, 2, 6, 4, 1, 7):
         wait(tg_of(k), ("tg", k))
         send(tg_of(k), tg_of(k), ("tgm",), mate)
 
@@ -284,9 +290,15 @@
     nza[0] = nzs[z]
     wait(nza.at[1:8], ("nza",))
     nyb[c, y] = nza[...]
+    nxa[x] = nxs[x]
+    wait(nxa.at[0:3], ("nxa",))
+    nyx[c, y] = nxa[...]
     for k in (4, 3, 5, 2, 6, 1, 7):
         send(nza, nyb.at[c, y], ("nyb",), yat(k))
     send(nza, nyb.at[c, y], ("nybm",), mate)
+    for k in (4, 3, 5, 2, 6, 1, 7):
+        send(nxa, nyx.at[c, y], ("nyx",), yat(k))
+    send(nxa, nyx.at[c, y], ("nyxm",), mate)
     phase("kproj")
 
     @pl.when(c == 0)
@@ -322,10 +334,6 @@
         xf_z(k, 2)
     for k in (1, 7):
         send(part.at[k], near.at[k // 7], ("near", k), zat(NZ - k))
-    phase("nyb")
-    wait(nyb.at[0, 0:7], ("nyb",))
-    for k in range(1, NY):
-        send(nyb.at[c, (y + k) % NY], nyb.at[c, (y + k) % NY], ("nybm",), mate)
     work(2)
     work(6)
     work(0)
@@ -358,6 +366,13 @@
     send(gout.at[1 - c], gin, ("gm",), mate)
     phase("zsend6")
     z_send(6)
+    phase("nyb")
+    wait(nyb.at[0, 0:7], ("nyb",))
+    for k in range(1, NY):
+        send(nyb.at[c, (y + k) % NY], nyb.at[c, (y + k) % NY], ("nybm",), mate)
+    wait(nyx.at[0, 0:7], ("nyx",))
+    for k in range(1, NY):
+        send(nyx.at[c, (y + k) % NY], nyx.at[c, (y + k) % NY], ("nyxm",), mate)
     phase("near")
     wait(near.at[0], ("near", 1))
     wait(near.at[1], ("near", 7))
@@ -378,6 +393,14 @@
     for j in range(4):
         pair = nr[2 * j : 2 * j + 2].reshape(128, 256)
         nrt[:, 128 * j : 128 * j + 128] = pair.T.astype(BF16)
+    wait(nyx.at[0], ("nyxm",))
+    for s in range(16):
+        rows = nyx[s % 2, s // 2].astype(F32)
+        for k in range(NX):
+            nrx[k, 4 * s : 4 * s + 4] = rows[k]
+    for j in range(2):
+        pair = nrx[2 * j : 2 * j + 2].reshape(128, 512)
+        nrtx[:, 128 * j : 128 * j + 128] = pair.T.astype(BF16)
     phase("gsum")
     wait(gin, ("gm",))
     for k in (4, 3, 5, 1, 7):
@@ -393,8 +416,10 @@
     for k in range(2, 7):
         total += zin[k].astype(F32)
     qflat = total.astype(BF16)
-    qz[0] = qflat
-
+    qz[0] = qflat[:, 0:128]
+    qx[x] = qflat[:, 128:256]
+    for e in (2, 1, 3):
+        send(qx.at[x], qx.at[x], ("qx",), xat(e))
     for k in (4, 3, 5, 2, 6, 1, 7):
         send(qz.at[0], qz.at[k], ("qz",), zat(k))
 
@@ -418,10 +443,14 @@
     for k in (4, 3, 5, 2, 6, 1, 7):
         send(nsum.at[(y + NY - k) % NY], nrecv.at[k], ("n",), yat(NY - k))
 
+    phase("wmat2")
+    wait(qx.at[0:3], ("qx",))
+    wz[...] = nn(nrtx[...], qx[...].reshape(256, 128)).astype(BF16).reshape(8, 64, 128)
+    for k in (4, 3, 5, 2, 6, 1, 7):
+        send(wz.at[(z + k) % NZ], wzin.at[k], ("wz",), zat(k))
     phase("wmat")
     wait(qz.at[1:8], ("qz",))
-    wsum = nn(nrt[...], qz[...].reshape(512, 256))
-    wpart[...] = wsum.astype(BF16).reshape(4, 64, 256)
+    wpart[...] = nn(nrt[...], qz[...].reshape(512, 128)).astype(BF16).reshape(4, 64, 128)
     for e in (2, 1, 3):
         send(wpart.at[(x + e) % NX], win.at[e], ("w",), xat(e))
 
@@ -446,7 +475,12 @@
     total = wpart[x].astype(F32)
     for e in range(1, NX):
         total += win[e].astype(F32)
-    wgrad_ref[...] = total
+    wgrad_ref[:, 0:128] = total
+    wait(wzin.at[1:8], ("wz",))
+    total = wz[z].astype(F32)
+    for k in range(1, NZ):
+        total += wzin[k].astype(F32)
+    wgrad_ref[:, 128:256] = total
 
     phase("sendwait")
     def sent_all(sem):
@@ -493,7 +527,9 @@
             buf(4, 2048), buf(16, 128), buf(64, 256), buf(1, 64), buf(4, 2048),
             buf(2, 8, 8, 2048), buf(64, 2048, dtype=F32), buf(64, 2048, dtype=F32),
             buf(8, 4, 256), buf(8, 4, 256), buf(2, 8, 8, 4, 256),
-            buf(8, 64, 256, dtype=F32), buf(256, 512), buf(2, 8, 16, 2048),
+            buf(8, 64, 256, dtype=F32), buf(256, 512),
+            buf(4, 4, 512), buf(4, 4, 512), buf(2, 8, 4, 4, 512), buf(4, 64, 512, dtype=F32), buf(512, 256),
+            buf(2, 8, 16, 2048),
             buf(2048, 256), buf(2048, 256), buf(2048, 256), buf(256, 2048),
             buf(8, 4, 72, 256), buf(8, 4, 64, 256),
             buf(256, 256), buf(256, 256),
@@ -501,7 +537,7 @@
             buf(8, 4, 64, 256), buf(2, 4, 64, 256),
             buf(8, 3, 64, 256),
             buf(8, 64, 256), buf(8, 64, 256),
-            buf(8, 64, 256), buf(4, 64, 256), buf(4, 64, 256),
+            buf(8, 64, 128), buf(4, 64, 128), buf(8, 64, 128), buf(8, 64, 128), buf(4, 64, 128), buf(4, 64, 128),
             buf(2, 8, 16, 2048), buf(8, 16, 2048), buf(8, 16, 2048), buf(3, 16, 2048), buf(8, 16, 2048),
             buf(2, 8, 8, 1024), buf(8, 8, 1024), buf(8, 8, 1024), buf(8, 8, 1024),
             buf(UNITS, 4, 256),

time: 70.4 us -> 69.3 us (0.984)
  the two profiles are of different devices: /device:TPU:8 before, /device:TPU:1 now
where the time goes in v6:
time: 69.3 us; the launch traced here: 68.7 us
  Pallas kernels  68 us (98%)
    pallas_call x1, Pallas kernels, body(): pl.pallas_call(kernel, out_shape=tuple((pltpu.VMEM(o.shape, o.dtype) for...  67.3 us

profile of v6, /device:TPU:1, one launch (start us, length us, event | category | flops | bytes accessed | tf_op | source)
XLA Modules:
  0.0 68.7 jit_solution(16093439208102217540)
XLA Ops:
  0.6 67.3 %shard_map.121 = (f32[4,2048]{1,0:T(4,128)S(1)}, f32[16,2048]{1,0:T(8,128)S(1)}, f32[64,256]{1,0:T(8,128)S(1)}) custom-call(bf16[4,2048]{1,0:T(4,128)(2,1)} %tr_hbm.1, bf16[16,2048]{1,0:T(8,128)(2,1)} %sr_hbm.1, bf16[16,128]{1,0:T(8,128)(2,1)} %bitcast.2, bf16[2048,256]{1,0:T(8,128)(2,1)} %wq_hbm.1, bf16[2048,256]{1,0:T(8,128)(2,1)} %wk_hbm.1, ...), custom_call_target="tpu_custom_call" | custom-call | tf_op jit(solution)/shard_map/pallas_call | solution.py:521
  68.0 0.7 %shard_map.122 = (f32[4,2048]{1,0:T(4,128)}, f32[16,2048]{1,0:T(8,128)}, f32[64,256]{1,0:T(8,128)}) custom-call(f32[4,2048]{1,0:T(4,128)S(1)} %get-tuple-element.6.a_ref, f32[16,2048]{1,0:T(8,128)S(1)} %get-tuple-element.7.b_ref, f32[64,256]{1,0:T(8,128)S(1)} %get-tuple-element.8.c_ref), custom_call_target="tpu_custom_call" | custom-call | tf_op jit(solution)/shard_map/pallas_call | solution.py:552

commit v7 on v6

--- a/solution.py
+++ b/solution.py
@@ -1,3 +1,4 @@
+import functools
 import math
 
 import jax
@@ -35,7 +36,7 @@
     tgrad_ref, sgrad_ref, wgrad_ref,
     tr, gn, sv, of, og,
     tg, xn, xo, nzs, nza, nyb, nr, nrt, nxs, nxa, nyx, nrx, nrtx, sg, wq, wk, wv, wo, zf, xf, kb, vb, dk, dv,
-    part, near, xin, zout, zin,
+    part, near, reli, relo, xin, zout, zin,
     qz, qx, wz, wzin, wpart, win,
     gout, gin, gsum, gmid, grecv, nout, nin, nsum, nrecv,
     units, ssem, rsem, lsem,
@@ -76,9 +77,9 @@
             names[name] = len(names)
         return names[name]
 
-    def send(src, dst, name, dev, sem=0):
+    def send(src, dst, name, dev, sem=0, count=1):
         assert size(src) % UNIT == 0
-        sent[sem] += size(src) // UNIT
+        sent[sem] += count * (size(src) // UNIT)
         pltpu.make_async_remote_copy(
             src_ref=src, dst_ref=dst, send_sem=ssem.at[sem], recv_sem=rsem.at[slot_of(name)],
             device_id=dev, device_id_type=MESH,
@@ -215,14 +216,29 @@
                     send(sg.at[1, 6], sg.at[1, 4], ("sg", 4), yat(6), 1)
                 send(sg.at[:, k], sg.at[:, k], ("sgm",), mate, 1)
 
+    back = {2: 3, 6: 1}
+
     def x_sends(k):
-        for e in (2, 1, 3):
-            send(part.at[k, (x + e) % NX], xin.at[k, e - 1], ("xin", k), xat(e))
+        e = back.get(k)
+        if e is None:
+            for e in (2, 1, 3):
+                send(part.at[k, (x + e) % NX], xin.at[k, e - 1], ("xin", k), xat(e))
+        else:
+            send(part.at[k, (x + 2) % NX], reli.at[k // 4], ("rel", k), xat(e))
+            send(part.at[k, (x + 4 - e) % NX], xin.at[k, 1], ("xin", k), xat(4 - e))
+
+    def x_relay(k):
+        e = back[k]
+        n = k // 4
+        wait(reli.at[n], ("rel", k))
+        relo[n] = (part[k, (x + e) % NX].astype(F32) + reli[n].astype(F32)).astype(BF16)
+        send(relo.at[n], xin.at[k, 0], ("xin", k), xat(e))
 
     def x_sum(k):
-        wait(xin.at[k], ("xin", k))
+        count = 2 if k in back else 3
+        wait(xin.at[k, 0:count], ("xin", k))
         total = part[k, x].astype(F32)
-        for n in range(3):
+        for n in range(count):
             total += xin[k, n].astype(F32)
         return total
 
@@ -343,6 +359,18 @@
     work(3)
     work(5)
     work(4)
+    x_relay(2)
+    x_relay(6)
+
+    def gsum_stage(count):
+        wait(gin, ("gm",))
+        for k in (4, 3, 5, 1, 7):
+            gsum[k] = (gout[c, k].astype(F32) + gin[k].astype(F32)).astype(BF16)
+        send(gsum.at[4], gmid.at[2], ("gmid",), yat((NY - 2 * way) % NY), count=count)
+        send(gsum.at[3], gmid.at[0], ("gmid",), yat(7), count=count)
+        send(gsum.at[5], gmid.at[1], ("gmid",), yat(1), count=count)
+        send(gsum.at[1], grecv.at[1], ("g",), yat(7), count=count)
+        send(gsum.at[7], grecv.at[7], ("g",), yat(1), count=count)
 
     phase("gmat1")
     dkb = dk[...].astype(BF16)
@@ -359,13 +387,9 @@
             )
 
     gmat(0)
-    phase("zsend2")
-    z_send(2)
     phase("gmat0")
     gmat(1)
     send(gout.at[1 - c], gin, ("gm",), mate)
-    phase("zsend6")
-    z_send(6)
     phase("nyb")
     wait(nyb.at[0, 0:7], ("nyb",))
     for k in range(1, NY):
@@ -378,12 +402,18 @@
     wait(near.at[1], ("near", 7))
     part[0] = (part[0].astype(F32) + near[0].astype(F32) + near[1].astype(F32)).astype(BF16)
     x_sends(0)
+    phase("gsumS")
+    pl.when(c == 0)(functools.partial(gsum_stage, 1))
     phase("zsend3")
     z_send(3)
     phase("zsend5")
     z_send(5)
     phase("zsend4")
     z_send(4)
+    phase("zsend2")
+    z_send(2)
+    phase("zsend6")
+    z_send(6)
     phase("nrt")
     wait(nyb.at[0], ("nybm",))
     for s in range(16):
@@ -401,15 +431,8 @@
     for j in range(2):
         pair = nrx[2 * j : 2 * j + 2].reshape(128, 512)
         nrtx[:, 128 * j : 128 * j + 128] = pair.T.astype(BF16)
-    phase("gsum")
-    wait(gin, ("gm",))
-    for k in (4, 3, 5, 1, 7):
-        gsum[k] = (gout[c, k].astype(F32) + gin[k].astype(F32)).astype(BF16)
-    send(gsum.at[4], gmid.at[2], ("gmid",), yat((NY - 2 * way) % NY))
-    send(gsum.at[3], gmid.at[0], ("gmid",), yat(7))
-    send(gsum.at[5], gmid.at[1], ("gmid",), yat(1))
-    send(gsum.at[1], grecv.at[1], ("g",), yat(7))
-    send(gsum.at[7], grecv.at[7], ("g",), yat(1))
+    phase("gsumN")
+    pl.when(c == 1)(functools.partial(gsum_stage, 0))
     phase("qflat")
     total = x_sum(0)
     wait(zin.at[2:7], ("zin",))
@@ -534,7 +557,7 @@
             buf(8, 4, 72, 256), buf(8, 4, 64, 256),
             buf(256, 256), buf(256, 256),
             buf(256, 256, dtype=F32), buf(256, 256, dtype=F32),
-            buf(8, 4, 64, 256), buf(2, 4, 64, 256),
+            buf(8, 4, 64, 256), buf(2, 4, 64, 256), buf(2, 64, 256), buf(2, 64, 256),
             buf(8, 3, 64, 256),
             buf(8, 64, 256), buf(8, 64, 256),
             buf(8, 64, 128), buf(4, 64, 128), buf(8, 64, 128), buf(8, 64, 128), buf(4, 64, 128), buf(4, 64, 128),

time: 69.3 us -> 69.2 us (level)
  no operation moved by 1% of the time
where the time goes in v7:
time: 69.2 us; the launch traced here: 69.1 us
  Pallas kernels  68.4 us (99%)
    pallas_call x1, Pallas kernels, body(): pl.pallas_call(kernel, out_shape=tuple((pltpu.VMEM(o.shape, o.dtype) for...  67.7 us

profile of v7, /device:TPU:1, one launch (start us, length us, event | category | flops | bytes accessed | tf_op | source)
XLA Modules:
  0.0 69.1 jit_solution(7489633841504485360)
XLA Ops:
  0.6 67.7 %shard_map.121 = (f32[4,2048]{1,0:T(4,128)S(1)}, f32[16,2048]{1,0:T(8,128)S(1)}, f32[64,256]{1,0:T(8,128)S(1)}) custom-call(bf16[4,2048]{1,0:T(4,128)(2,1)} %tr_hbm.1, bf16[16,2048]{1,0:T(8,128)(2,1)} %sr_hbm.1, bf16[16,128]{1,0:T(8,128)(2,1)} %bitcast.2, bf16[2048,256]{1,0:T(8,128)(2,1)} %wq_hbm.1, bf16[2048,256]{1,0:T(8,128)(2,1)} %wk_hbm.1, ...), custom_call_target="tpu_custom_call" | custom-call | tf_op jit(solution)/shard_map/pallas_call | solution.py:544
  68.4 0.7 %shard_map.122 = (f32[4,2048]{1,0:T(4,128)}, f32[16,2048]{1,0:T(8,128)}, f32[64,256]{1,0:T(8,128)}) custom-call(f32[4,2048]{1,0:T(4,128)S(1)} %get-tuple-element.6.a_ref, f32[16,2048]{1,0:T(8,128)S(1)} %get-tuple-element.7.b_ref, f32[64,256]{1,0:T(8,128)S(1)} %get-tuple-element.8.c_ref), custom_call_target="tpu_custom_call" | custom-call | tf_op jit(solution)/shard_map/pallas_call | solution.py:575
